TPU v7x, 256 devices: a 2x2x32 block of a 4x8x32 slice. The times are simulated.
256 devices in a mesh: grp: 4 (over y, x), ep: 32 (over z), tp: 2 (over core).
Axes of the slice: x: 2, y: 2, z: 32, core: 2. Of those that a mesh axis runs over, the one named last changes fastest.
The devices are a block of a 4x8x32 slice.
Arguments:
- tokens: bfloat16 [65536, 2048], P(('grp', 'ep', 'tp')), parts along dimension 0, may hold values from -6 to 6
- norm_gain: float32 [2048], replicated, may hold values from 0.1 to 1.9
- expert_ids: int32 [65536, 2], P(('grp', 'ep', 'tp')), parts along dimension 0, may hold values from 0 to 31, all different within a row; in each aligned block of 256 rows (0 to 255, 256 to 511, ...) at most 24 rows name the same one
- route_weights: float32 [65536, 2], P(('grp', 'ep', 'tp')), parts along dimension 0, may hold values from 0.05 to 1
- w_gate: bfloat16 [32, 2048, 1024], P('ep', None, 'tp'), may hold values from -0.125 to 0.125
- w_up: bfloat16 [32, 2048, 1024], P('ep', None, 'tp'), may hold values from -0.125 to 0.125
- w_down: bfloat16 [32, 1024, 2048], P('ep', 'tp'), may hold values from -0.1875 to 0.1875
Outputs:
- mixed: bfloat16 [65536, 2048], P(('grp', 'ep', 'tp')), parts along dimension 0
There are 4 independent parts, one for each index of `grp`. A program takes and returns all parts, laid end to end along the dimension named above; an argument that names none is the same for every part. Nothing has to cross between parts.
Inputs may be any that keep to these rules, and one draw needn't show every extreme that they name: `expert_ids`: each row names 2 different experts. Among the rows of one device no expert is named more than 24 times, and in every draw some expert is named exactly 24 times by the rows of some device.
All inputs are finite; a program needn't handle non-finite values.
Results may differ from a plain program's by a relative error of at most 0.0071.
Values may be sent and summed in bfloat16 or wider, within the bound.
No kernel may reach another device: no remote copies, remote signals or barrier semaphores. Data moves between devices by JAX's collectives and lax.ppermute only.
A program may use at most 128 MiB of HBM per device.

v0:
```python
import jax
import jax.numpy as jnp
from jax import lax
from jax.sharding import PartitionSpec as P


def in_one_piece(arrays, axis, dim, along):
    ends, at = ([], 0)
    for a in arrays[:-1]:
        at += a.shape[along]
        ends.append(at)
    both = jnp.concatenate(arrays, axis=along)
    return tuple(jnp.split(lax.all_gather(both, axis, axis=dim, tiled=True), ends, axis=along))


def per_device(tokens, norm_gain, expert_ids, route_weights, w_gate, w_up, w_down):
    tok_rows = tokens.shape[0]
    top_count = expert_ids.shape[1]
    width = tokens.shape[1]
    local_experts = w_gate.shape[0]
    ep_size = lax.axis_size("ep")
    experts = local_experts * ep_size
    slots = 3 * tok_rows * top_count // (2 * experts)
    values = tokens.astype(jnp.float32)
    scale = lax.rsqrt(jnp.mean(values * values, axis=-1, keepdims=True) + 1e-06)
    normed = (values * scale * norm_gain).astype(jnp.bfloat16)
    flat_ids = expert_ids.reshape(-1)
    onehot = (flat_ids[:, None] == jnp.arange(experts, dtype=jnp.int32)[None, :]).astype(jnp.int32)
    before = jnp.cumsum(onehot, axis=0) - onehot
    slot_of = jnp.sum(before * onehot, axis=1)
    target = flat_ids * slots + slot_of
    owner = jnp.arange(tok_rows * top_count, dtype=jnp.int32) // top_count + 1
    source = jnp.zeros((experts * slots,), jnp.int32).at[target].set(owner)
    filled = source > 0
    picked = jnp.take(normed, jnp.maximum(source - 1, 0), axis=0)
    outgoing = jnp.where(filled[:, None], picked, jnp.zeros_like(picked))
    outgoing = outgoing.reshape(ep_size, local_experts, slots, width)
    gate_full, up_full = in_one_piece((w_gate, w_up), "tp", 2, 0)
    down_full = lax.all_gather(w_down, "tp", axis=1, tiled=True)
    arrived = lax.all_to_all(outgoing, "ep", split_axis=0, concat_axis=0, tiled=True)
    senders, _, part_slots, _ = arrived.shape
    rows = jnp.transpose(arrived, (1, 0, 2, 3)).reshape(local_experts, senders * part_slots, width)
    gate = jnp.einsum("erd,edf->erf", rows, gate_full, preferred_element_type=jnp.float32)
    upper = jnp.einsum("erd,edf->erf", rows, up_full, preferred_element_type=jnp.float32)
    hidden = (jax.nn.silu(gate) * upper).astype(jnp.bfloat16)
    result = jnp.einsum(
        "erf,efd->erd", hidden, down_full, preferred_element_type=jnp.float32
    ).astype(jnp.bfloat16)
    result = result.reshape(local_experts, senders, part_slots, width)
    result = jnp.transpose(result, (1, 0, 2, 3))
    results = lax.all_to_all(result, "ep", split_axis=0, concat_axis=0, tiled=True)
    results = results.reshape(experts * slots, width)
    gathered = jnp.take(results, target, axis=0).reshape(tok_rows, top_count, width)
    mixed = jnp.sum(route_weights[:, :, None] * gathered.astype(jnp.float32), axis=1)
    return mixed.astype(jnp.bfloat16)


def solution(mesh):
    in_specs = (
        P(("grp", "ep", "tp"), None),
        P(),
        P(("grp", "ep", "tp"), None),
        P(("grp", "ep", "tp"), None),
        P("ep", None, "tp"),
        P("ep", None, "tp"),
        P("ep", "tp", None),
    )
    out_specs = P(("grp", "ep", "tp"), None)
    return jax.shard_map(
        per_device, mesh=mesh, in_specs=in_specs, out_specs=out_specs, check_vma=False
    )
```

profile of v0, /device:TPU:359, one launch (start us, length us, event | category | flops | bytes accessed | tf_op | source)
XLA Modules:
  0.0 670.5 jit_solution(12743148507947471114)
XLA Ops:
  6.5 0.8 copy.23
  7.4 0.1 eq.26
  7.5 0.1 reshape.138
  7.7 0.7 broadcast_multiply_fusion
  8.4 1.2 reduce-window.6
  9.5 0.2 slice_reduce_fusion
  9.8 0.1 copy.28
  9.9 0.1 mul.62
  10.1 0.1 fusion.12
  10.2 2.4 scatter_custom_fusion
  12.7 0.1 broadcast_in_dim.44
  12.8 0.1 broadcast_in_dim.46
  12.9 1.5 fusion.7
  14.4 1.5 fusion.9
  16.0 4.3 gather_fusion
  20.2 3.3 select_select_fusion
  23.6 28.7 %all-to-all-start = ((bf16[32,1,24,2048]{3,2,1,0:T(8,128)(2,1)}), bf16[32,1,24,2048]{3,2,1,0:T(8,128)(2,1)S(1)}, u32[]{:S(2)}, u32[]{:S(2)}) async-start(bf16[32,1,24,2048]{3,2,1,0:T(8,128)(2,1)} %select_select_fusion), calls=%async_computation | async-start | bytes 6291456 | tf_op jit(solution)/shard_map/all_to_all | solution.py:40
  52.3 0.1 all-gather.3.cloned.1.call-start
  52.3 4.6 pad_maximum_fusion
  56.9 0.1 all-gather.3.cloned.1.call-update
  57.0 0.1 all-gather.5.cloned.1.call-start
  57.0 0.7 all-gather.5.cloned.1.call-update
  57.8 38.3 %all-gather.3.cloned.1.call-done = bf16[2,2048,1024]{2,1,0:T(8,128)(2,1)} async-done(((bf16[2,2048,512]{2,1,0:T(8,128)(2,1)}), bf16[2,2048,1024]{2,1,0:T(8,128)(2,1)}) %all-gather.3.cloned.1.call-update) | async-done | bytes 8388624 | tf_op jit(solution)/shard_map/all_gather | solution.py:13
  96.1 240.6 %all-to-all-done = bf16[32,1,24,2048]{3,2,1,0:T(8,128)(2,1)S(1)} async-done(((bf16[32,1,24,2048]{3,2,1,0:T(8,128)(2,1)}), bf16[32,1,24,2048]{3,2,1,0:T(8,128)(2,1)S(1)}, u32[]{:S(2)}, u32[]{:S(2)}) %all-to-all-start) | async-done | bytes 3145760 | tf_op jit(solution)/shard_map/all_to_all | solution.py:40
  336.6 0.0 copy-start.2
  336.6 5.3 fusion
  342.0 0.0 copy-done.2
  342.0 5.0 multiply_convert_fusion
  347.0 0.0 all-gather.5.cloned.1.call-done
  347.0 7.7 %fusion.4 = bf16[768,2048]{1,0:T(8,128)(2,1)} fusion(bf16[768,1024]{1,0:T(8,128)(2,1)} %multiply_convert_fusion, bf16[1,1024,2048]{2,1,0:T(8,128)(2,1)} %all-gather.5.cloned.1.call-done), kind=kOutput, calls=%fused_computation.12 | convolution fusion | flops 3222798336 | bytes 8912896 | tf_op jit(solution)/shard_map/erf,efd->erd/dot_general | solution.py:46
  354.8 0.0 copy-start
  354.8 0.0 copy-start.1
  354.8 8.7 %all-to-all-start.1 = ((bf16[32,1,24,2048]{3,2,1,0:T(8,128)(2,1)}), bf16[32,1,24,2048]{3,2,1,0:T(8,128)(2,1)S(1)}, u32[]{:S(2)}, u32[]{:S(2)}) async-start(bf16[32,1,24,2048]{3,2,1,0:T(8,128)(2,1)} %bitcast.49), calls=%async_computation.1 | async-start | bytes 6291456 | tf_op jit(solution)/shard_map/all_to_all | solution.py:51
  363.5 0.1 reduce_sum.32
  363.6 0.1 copy.26
  363.7 0.0 copy-done
  363.7 0.2 copy.27
  363.9 0.0 copy-done.1
  363.9 0.1 copy.22
  364.0 283.8 %all-to-all-done.1 = bf16[32,1,24,2048]{3,2,1,0:T(8,128)(2,1)S(1)} async-done(((bf16[32,1,24,2048]{3,2,1,0:T(8,128)(2,1)}), bf16[32,1,24,2048]{3,2,1,0:T(8,128)(2,1)S(1)}, u32[]{:S(2)}, u32[]{:S(2)}) %all-to-all-start.1) | async-done | bytes 3145760 | tf_op jit(solution)/shard_map/all_to_all | solution.py:51
  647.9 3.3 gather_fusion.1
  651.2 3.2 gather.15
  654.4 9.2 %multiply_reduce_fusion = bf16[256,2048]{1,0:T(8,128)(2,1)} fusion(bf16[256,2,2048]{2,1,0:T(2,128)(2,1)S(1)} %gather.15, pred[256,2]{1,0:T(8,128)(4,1)S(1)} %copy.27, f32[256,2]{1,0:T(8,128)S(1)} %copy.22), kind=kLoop, calls=%fused_computation.10 | loop fusion | flops 3670016 | bytes 3148288 | tf_op jit(solution)/shard_map/reduce_sum | solution.py:54
  (11 shorter events, 0.1 us)
Async XLA Ops:
  23.6 313.1 %all-to-all-start = ((bf16[32,1,24,2048]{3,2,1,0:T(8,128)(2,1)}), bf16[32,1,24,2048]{3,2,1,0:T(8,128)(2,1)S(1)}, u32[]{:S(2)}, u32[]{:S(2)}) async-start(bf16[32,1,24,2048]{3,2,1,0:T(8,128)(2,1)} %select_select_fusion), calls=%async_computation | async-start | bytes 6291456 | tf_op jit(solution)/shard_map/all_to_all | solution.py:40
  52.3 43.8 %all-gather.3.cloned.1.call-start = ((), (), s32[]{:S(2)}) async-start(), calls=%async_computation.2 | async-start | bytes 12582912 | tf_op jit(solution)/shard_map/all_gather | solution.py:13
  57.0 290.1 %all-gather.5.cloned.1.call-start = ((), (), s32[]{:S(2)}) async-start(), calls=%async_computation.3 | async-start | bytes 6291456 | tf_op jit(solution)/shard_map/all_gather | solution.py:39
  336.6 5.4 copy-start.2
  354.8 8.9 %copy-start = (s32[256,2]{0,1:T(2,128)S(1)}, s32[256,2]{0,1:T(2,128)}, u32[]{:S(2)}) copy-start(s32[256,2]{0,1:T(2,128)} %param.9) | copy-start | bytes 6148
  354.8 9.1 %copy-start.1 = (f32[256,2]{0,1:T(2,128)S(1)}, f32[256,2]{0,1:T(2,128)}, u32[]{:S(2)}) copy-start(f32[256,2]{0,1:T(2,128)} %param.10) | copy-start | bytes 6148
  354.8 293.1 %all-to-all-start.1 = ((bf16[32,1,24,2048]{3,2,1,0:T(8,128)(2,1)}), bf16[32,1,24,2048]{3,2,1,0:T(8,128)(2,1)S(1)}, u32[]{:S(2)}, u32[]{:S(2)}) async-start(bf16[32,1,24,2048]{3,2,1,0:T(8,128)(2,1)} %bitcast.49), calls=%async_computation.1 | async-start | bytes 6291456 | tf_op jit(solution)/shard_map/all_to_all | solution.py:51
Sparse Core Ops, SparseCore 0:
  57.1 38.9 all-gather.2
  97.9 31.8 all-gather.4
where the time goes:
time: 671 us; the launch traced here: 670 us
  waiting for transfers between devices  563 us (84%)
  starting transfers between devices  37.5 us (6%)
  other arithmetic  22.2 us (3%)
  matrix products  18.1 us (3%)
  local copies, waits for them, and re-layouts  15.5 us (2%)
  between operations  13.6 us (2%)
    all_to_all x1, waiting for transfers between devices, per_device(): lax.all_to_all(result, 'ep', split_axis=0, concat_axis=0, tiled=True)  284 us
    all_to_all x1, waiting for transfers between devices, per_device(): lax.all_to_all(outgoing, 'ep', split_axis=0, concat_axis=0, tiled=True)  241 us
    all_gather x1, waiting for transfers between devices, in_one_piece(): lax.all_gather(both, axis, axis=dim, tiled=True)  38.3 us
    all_to_all x1, starting transfers between devices, per_device(): lax.all_to_all(outgoing, 'ep', split_axis=0, concat_axis=0, tiled=True)  28.7 us
  transfers between devices with their start and end apart: 4, of which 3 were waited for; matrix products, arithmetic and copies ran while one was open for 2% of the time, Pallas kernels for 0%

commit v1 on v0

v1 whole, which is shorter than its diff:
```python
import jax
import jax.numpy as jnp
from jax import lax
from jax.experimental import pallas as pl
from jax.experimental.pallas import tpu as pltpu
from jax.sharding import PartitionSpec as P


F32, BF16, I32 = jnp.float32, jnp.bfloat16, jnp.int32
VMEM = pl.BlockSpec(memory_space=pltpu.VMEM)
SMEM = pl.BlockSpec(memory_space=pltpu.SMEM)
MIB = 1 << 20


def dot(a, b):
    return jnp.dot(a, b, preferred_element_type=F32)


def one_hot(pick):
    return pick.astype(F32).astype(BF16)


def place_kernel(experts, slots, me_ref, ids_ref, tokens_ref, gain_ref, pos_ref, send_ref):
    rows = tokens_ref.shape[0]
    values = tokens_ref[...].astype(F32)
    scale = lax.rsqrt(jnp.mean(values * values, axis=-1, keepdims=True) + 1e-06)
    normed = (values * scale * gain_ref[...]).astype(BF16)
    earlier = one_hot(
        lax.broadcasted_iota(I32, (rows, rows), 0) < lax.broadcasted_iota(I32, (rows, rows), 1)
    )
    names = lax.broadcasted_iota(I32, (experts, rows), 0)
    taken = jnp.zeros((experts, 1), F32)
    places = []
    for k in range(ids_ref.shape[0]):
        ids = ids_ref[k : k + 1, :]
        hot = (names == ids).astype(F32)
        before = dot(hot.astype(BF16), earlier) + taken
        taken = taken + jnp.sum(hot, axis=1, keepdims=True)
        slot = jnp.sum(hot * before, axis=0, keepdims=True).astype(I32)
        away = ids - me_ref[0]
        away = jnp.where(away < 0, away + experts, away)
        near = jnp.where(2 * away <= experts, 2 * away - 1, 2 * (experts - away))
        near = jnp.where(away == 0, 0, near)
        pos = near * slots + slot
        pos_ref[k : k + 1, :] = pos
        places.append(pos)
    chunk = 128
    for start in range(0, experts * slots, chunk):
        at = lax.broadcasted_iota(I32, (chunk, rows), 0) + start
        pick = at == places[0]
        for pos in places[1:]:
            pick = pick | (at == pos)
        send_ref[start : start + chunk, :] = dot(one_hot(pick), normed).astype(BF16)


def weigh(start, pos_ref, weights_ref, parts):
    rows = jnp.concatenate([p[...] for p in parts], axis=0)
    total = None
    for k in range(pos_ref.shape[1]):
        at = lax.broadcasted_iota(I32, (pos_ref.shape[0], rows.shape[0]), 1) + start
        pick = one_hot(at == pos_ref[:, k : k + 1])
        part = weights_ref[:, k : k + 1] * dot(pick, rows)
        total = part if total is None else total + part
    return total


def first_mix_kernel(pos_ref, weights_ref, *refs):
    refs[-1][...] = weigh(0, pos_ref, weights_ref, refs[:-1])


def last_mix_kernel(start, pos_ref, weights_ref, sofar_ref, *refs):
    refs[-1][...] = (sofar_ref[...] + weigh(start, pos_ref, weights_ref, refs[:-1])).astype(BF16)


def call(kernel, out, operands, limit, specs=None):
    return pl.pallas_call(
        kernel,
        out_shape=out,
        in_specs=specs or [VMEM] * len(operands),
        out_specs=jax.tree.map(lambda _: VMEM, out),
        compiler_params=pltpu.CompilerParams(vmem_limit_bytes=limit * MIB),
    )(*operands)


def per_device(tokens, norm_gain, expert_ids, route_weights, w_gate, w_up, w_down):
    tok_rows, width = tokens.shape
    top_count = expert_ids.shape[1]
    ep_size, tp_size = lax.axis_size("ep"), lax.axis_size("tp")
    experts = w_gate.shape[0] * ep_size
    slots = 3 * tok_rows * top_count // (2 * experts)

    def sds(shape, dtype):
        return jax.ShapeDtypeStruct(shape, dtype)

    order = [0]
    for d in range(1, ep_size // 2 + 1):
        order += [d] if 2 * d == ep_size else [d, -d]
    first = 2 * 11 + 1

    me = lax.axis_index("ep").astype(I32)[None]
    pos, send = call(
        lambda *refs: place_kernel(experts, slots, *refs),
        (sds((top_count, tok_rows), I32), sds((experts * slots, width), BF16)),
        (me, expert_ids.T, tokens, norm_gain[None, :]),
        24,
        [SMEM, VMEM, VMEM, VMEM],
    )

    swap = [(i, (i + 1) % tp_size) for i in range(tp_size)]

    def whole(w, axis):
        return jnp.concatenate([w, lax.ppermute(w, "tp", swap)], axis=axis)

    def shift(rows, d):
        if d == 0:
            return rows
        return lax.ppermute(rows, "ep", [(i, (i + d) % ep_size) for i in range(ep_size)])

    gate_full, up_full, down_full = whole(w_gate[0], 1), whole(w_up[0], 1), whole(w_down[0], 0)

    def expert(rows):
        hidden = (jax.nn.silu(dot(rows, gate_full)) * dot(rows, up_full)).astype(BF16)
        return dot(hidden, down_full).astype(BF16)

    arrived = []
    for i, d in enumerate(order):
        arrived.append(shift(send[i * slots : (i + 1) * slots], d))
    back, result = [], None
    for lo, hi in ((0, first), (first, len(order))):
        if result is not None:
            arrived, _ = lax.optimization_barrier((arrived, result))
        result = expert(jnp.concatenate(arrived[lo:hi], axis=0))
        back += [shift(result[i * slots : (i + 1) * slots], -d) for i, d in enumerate(order[lo:hi])]
    cols = pos.T
    sofar = call(
        first_mix_kernel,
        sds((tok_rows, width), F32),
        (cols, route_weights, *back[:first]),
        24,
    )
    return call(
        lambda *refs: last_mix_kernel(first * slots, *refs),
        sds((tok_rows, width), BF16),
        (cols, route_weights, sofar, *back[first:]),
        24,
    )


def solution(mesh):
    in_specs = (
        P(("grp", "ep", "tp"), None),
        P(),
        P(("grp", "ep", "tp"), None),
        P(("grp", "ep", "tp"), None),
        P("ep", None, "tp"),
        P("ep", None, "tp"),
        P("ep", "tp", None),
    )
    out_specs = P(("grp", "ep", "tp"), None)

    return jax.shard_map(
        per_device, mesh=mesh, in_specs=in_specs, out_specs=out_specs, check_vma=False
    )
```

time: 671 us -> 659 us (0.982)
  the two profiles are of different devices: /device:TPU:359 before, /device:TPU:103 now
where the time goes in v1:
time: 659 us; the launch traced here: 651 us
  starting transfers between devices  417 us (63%)
  waiting for transfers between devices  191 us (29%)
  matrix products  24.3 us (4%)
  local copies, waits for them, and re-layouts  13.2 us (2%)
    ppermute x62, starting transfers between devices, shift(): lax.ppermute(rows, 'ep', [(i, (i + d) % ep_size) for i in range(ep_size)])  412 us
    ppermute x62, waiting for transfers between devices, shift(): lax.ppermute(rows, 'ep', [(i, (i + d) % ep_size) for i in range(ep_size)])  191 us
    dot_general x4, matrix products, dot(): return jnp.dot(a, b, preferred_element_type=F32)  24.3 us
  transfers between devices with their start and end apart: 65, of which 16 were waited for; matrix products, arithmetic and copies ran while one was open for 2% of the time, Pallas kernels for 0%

profile of v1, /device:TPU:103, one launch (start us, length us, event | category | flops | bytes accessed | tf_op | source)
XLA Modules:
  0.0 650.8 jit_solution(6450588973955935002)
XLA Ops:
  4.1 2.0 collective-permute-start
  6.1 4.6 collective-permute-start.2
  10.7 17.1 %collective-permute-start.3 = (bf16[24,2048]{1,0:T(8,128)(2,1)S(1)}, bf16[24,2048]{1,0:T(8,128)(2,1)S(1)}, u32[]{:S(2)}, u32[]{:S(2)}) collective-permute-start(bf16[24,2048]{1,0:T(8,128)(2,1)S(1)} %get-tuple-element.54), channel_id=1, source_target_pairs={{0,60},{2,62},{4,0},{6,2},{8,4},{10,6},{12,8},{14,10},{16,12},{18,... | collective-permute-start | bytes 294920 | tf_op jit(solution)/shard_map/ppermute | solution.py:117
  28.6 4.5 collective-permute-start.5
  33.2 5.4 collective-permute-start.7
  38.8 6.3 collective-permute-start.9
  45.5 2.2 collective-permute-done.6
  47.7 7.9 %collective-permute-start.11 = (bf16[24,2048]{1,0:T(8,128)(2,1)S(1)}, bf16[24,2048]{1,0:T(8,128)(2,1)S(1)}, u32[]{:S(2)}, u32[]{:S(2)}) collective-permute-start(bf16[24,2048]{1,0:T(8,128)(2,1)S(1)} %get-tuple-element.46), channel_id=1, source_target_pairs={{0,52},{2,54},{4,56},{6,58},{8,60},{10,62},{12,0},{14,2},{16,4},{1... | collective-permute-start | bytes 294920 | tf_op jit(solution)/shard_map/ppermute | solution.py:117
  55.5 4.2 collective-permute-start.12
  59.7 5.7 collective-permute-start.13
  65.4 6.2 collective-permute-start.14
  71.6 4.2 collective-permute-start.15
  75.9 5.0 collective-permute-start.16
  80.9 15.3 %collective-permute-done.12 = bf16[24,2048]{1,0:T(8,128)(2,1)S(1)} collective-permute-done((bf16[24,2048]{1,0:T(8,128)(2,1)S(1)}, bf16[24,2048]{1,0:T(8,128)(2,1)S(1)}, u32[]{:S(2)}, u32[]{:S(2)}) %collective-permute-start.12) | collective-permute-done | bytes 98336 | tf_op jit(solution)/shard_map/ppermute | solution.py:117
  97.8 3.2 collective-permute-start.22
  101.2 23.8 %collective-permute-done.16 = bf16[24,2048]{1,0:T(8,128)(2,1)S(1)} collective-permute-done((bf16[24,2048]{1,0:T(8,128)(2,1)S(1)}, bf16[24,2048]{1,0:T(8,128)(2,1)S(1)}, u32[]{:S(2)}, u32[]{:S(2)}) %collective-permute-start.16) | collective-permute-done | bytes 98336 | tf_op jit(solution)/shard_map/ppermute | solution.py:117
  125.0 13.3 %collective-permute-start.19 = (bf16[24,2048]{1,0:T(8,128)(2,1)S(1)}, bf16[24,2048]{1,0:T(8,128)(2,1)S(1)}, u32[]{:S(2)}, u32[]{:S(2)}) collective-permute-start(bf16[24,2048]{1,0:T(8,128)(2,1)S(1)} %get-tuple-element.38), channel_id=1, source_target_pairs={{0,44},{2,46},{4,48},{6,50},{8,52},{10,54},{12,56},{14,58},{16,60}... | collective-permute-start | bytes 294920 | tf_op jit(solution)/shard_map/ppermute | solution.py:117
  138.3 12.5 %collective-permute-done.18 = bf16[24,2048]{1,0:T(8,128)(2,1)S(1)} collective-permute-done((bf16[24,2048]{1,0:T(8,128)(2,1)S(1)}, bf16[24,2048]{1,0:T(8,128)(2,1)S(1)}, u32[]{:S(2)}, u32[]{:S(2)}) %collective-permute-start.18) | collective-permute-done | bytes 98336 | tf_op jit(solution)/shard_map/ppermute | solution.py:117
  152.7 12.4 %collective-permute-start.21 = (bf16[24,2048]{1,0:T(8,128)(2,1)S(1)}, bf16[24,2048]{1,0:T(8,128)(2,1)S(1)}, u32[]{:S(2)}, u32[]{:S(2)}) collective-permute-start(bf16[24,2048]{1,0:T(8,128)(2,1)S(1)} %get-tuple-element.36), channel_id=1, source_target_pairs={{0,42},{2,44},{4,46},{6,48},{8,50},{10,52},{12,54},{14,56},{16,58}... | collective-permute-start | bytes 294920 | tf_op jit(solution)/shard_map/ppermute | solution.py:117
  165.1 16.1 %collective-permute-done.20 = bf16[24,2048]{1,0:T(8,128)(2,1)S(1)} collective-permute-done((bf16[24,2048]{1,0:T(8,128)(2,1)S(1)}, bf16[24,2048]{1,0:T(8,128)(2,1)S(1)}, u32[]{:S(2)}, u32[]{:S(2)}) %collective-permute-start.20) | collective-permute-done | bytes 98336 | tf_op jit(solution)/shard_map/ppermute | solution.py:117
  181.3 14.9 %collective-permute-start.48 = (bf16[24,2048]{1,0:T(8,128)(2,1)S(1)}, bf16[24,2048]{1,0:T(8,128)(2,1)S(1)}, u32[]{:S(2)}, u32[]{:S(2)}) collective-permute-start(bf16[24,2048]{1,0:T(8,128)(2,1)S(1)} %get-tuple-element.34), channel_id=1, source_target_pairs={{0,40},{2,42},{4,44},{6,46},{8,48},{10,50},{12,52},{14,54},{16,56}... | collective-permute-start | bytes 294920 | tf_op jit(solution)/shard_map/ppermute | solution.py:117
  196.3 3.8 collective-permute-done.47
  200.0 18.0 %collective-permute-start.49 = (bf16[24,2048]{1,0:T(8,128)(2,1)S(1)}, bf16[24,2048]{1,0:T(8,128)(2,1)S(1)}, u32[]{:S(2)}, u32[]{:S(2)}) collective-permute-start(bf16[24,2048]{1,0:T(8,128)(2,1)S(1)} %get-tuple-element.33), channel_id=1, source_target_pairs={{0,26},{2,28},{4,30},{6,32},{8,34},{10,36},{12,38},{14,40},{16,42}... | collective-permute-start | bytes 294920 | tf_op jit(solution)/shard_map/ppermute | solution.py:117
  218.5 3.9 fusion.2
  222.4 5.1 collective-permute-done.48
  227.5 13.9 %collective-permute-start.51 = (bf16[24,2048]{1,0:T(8,128)(2,1)}, bf16[24,2048]{1,0:T(8,128)(2,1)S(1)}, u32[]{:S(2)}, u32[]{:S(2)}) collective-permute-start(bf16[24,2048]{1,0:T(8,128)(2,1)} %get-tuple-element.31), channel_id=1, source_target_pairs={{0,28},{2,30},{4,32},{6,34},{8,36},{10,38},{12,40},{14,42},{16,44}... | collective-permute-start | bytes 294920 | tf_op jit(solution)/shard_map/ppermute | solution.py:117
  241.4 4.0 collective-permute-start.52
  245.5 8.6 %collective-permute-start.53 = (bf16[24,2048]{1,0:T(8,128)(2,1)S(1)}, bf16[24,2048]{1,0:T(8,128)(2,1)S(1)}, u32[]{:S(2)}, u32[]{:S(2)}) collective-permute-start(bf16[24,2048]{1,0:T(8,128)(2,1)S(1)} %get-tuple-element.29), channel_id=1, source_target_pairs={{0,30},{2,32},{4,34},{6,36},{8,38},{10,40},{12,42},{14,44},{16,46}... | collective-permute-start | bytes 294920 | tf_op jit(solution)/shard_map/ppermute | solution.py:117
  254.1 10.3 %collective-permute-start.54 = (bf16[24,2048]{1,0:T(8,128)(2,1)S(1)}, bf16[24,2048]{1,0:T(8,128)(2,1)S(1)}, u32[]{:S(2)}, u32[]{:S(2)}) collective-permute-start(bf16[24,2048]{1,0:T(8,128)(2,1)S(1)} %get-tuple-element.28), channel_id=1, source_target_pairs={{0,34},{2,36},{4,38},{6,40},{8,42},{10,44},{12,46},{14,48},{16,50}... | collective-permute-start | bytes 294920 | tf_op jit(solution)/shard_map/ppermute | solution.py:117
  265.8 5.7 collective-permute-start.55
  271.5 9.8 %convolution_convert_fusion = bf16[552,2048]{1,0:T(8,128)(2,1)S(1)} fusion(bf16[512,2048]{1,0:T(8,128)(2,1)} %copy-done.11, bf16[512,2048]{1,0:T(8,128)(2,1)} %bitcast.18, f32[552,1024]{1,0:T(8,128)} %fusion.2, bf16[552,2048]{1,0:T(8,128)(2,1)} %copy-done.4, bf16[2048,512]{1,0:T(8,128)(2,1)} %copy-done.10, bf16[2048,512]{1,0:T(8,128)(2,1)} %bitcast.21), kind=kOutput, calls=%fused_computation.3 | convolution fusion | flops 4651810816 | bytes 15171584 | tf_op jit(solution)/shard_map/dot_general | solution.py:16
  281.3 24.2 %collective-permute-done.51 = bf16[24,2048]{1,0:T(8,128)(2,1)S(1)} collective-permute-done((bf16[24,2048]{1,0:T(8,128)(2,1)}, bf16[24,2048]{1,0:T(8,128)(2,1)S(1)}, u32[]{:S(2)}, u32[]{:S(2)}) %collective-permute-start.51) | collective-permute-done | bytes 98336 | tf_op jit(solution)/shard_map/ppermute | solution.py:117
  305.6 17.6 %collective-permute-done.54 = bf16[24,2048]{1,0:T(8,128)(2,1)S(1)} collective-permute-done((bf16[24,2048]{1,0:T(8,128)(2,1)S(1)}, bf16[24,2048]{1,0:T(8,128)(2,1)S(1)}, u32[]{:S(2)}, u32[]{:S(2)}) %collective-permute-start.54) | collective-permute-done | bytes 98336 | tf_op jit(solution)/shard_map/ppermute | solution.py:117
  329.0 4.5 fusion.1
  333.5 6.0 fusion.5
  340.3 4.4 collective-permute-start.56
  344.7 13.6 %collective-permute-start.57 = (bf16[24,2048]{1,0:T(8,128)(2,1)S(1)}, bf16[24,2048]{1,0:T(8,128)(2,1)S(1)}, u32[]{:S(2)}, u32[]{:S(2)}) collective-permute-start(bf16[24,2048]{1,0:T(8,128)(2,1)S(1)} %get-tuple-element.89), channel_id=1, source_target_pairs={{0,24},{2,26},{4,28},{6,30},{8,32},{10,34},{12,36},{14,38},{16,40}... | collective-permute-start | bytes 294920 | tf_op jit(solution)/shard_map/ppermute | solution.py:117
  358.3 5.2 collective-permute-start.58
  363.5 10.7 %collective-permute-start.59 = (bf16[24,2048]{1,0:T(8,128)(2,1)S(1)}, bf16[24,2048]{1,0:T(8,128)(2,1)S(1)}, u32[]{:S(2)}, u32[]{:S(2)}) collective-permute-start(bf16[24,2048]{1,0:T(8,128)(2,1)S(1)} %get-tuple-element.87), channel_id=1, source_target_pairs={{0,26},{2,28},{4,30},{6,32},{8,34},{10,36},{12,38},{14,40},{16,42}... | collective-permute-start | bytes 294920 | tf_op jit(solution)/shard_map/ppermute | solution.py:117
  374.3 12.1 %collective-permute-start.28 = (bf16[24,2048]{1,0:T(8,128)(2,1)S(1)}, bf16[24,2048]{1,0:T(8,128)(2,1)S(1)}, u32[]{:S(2)}, u32[]{:S(2)}) collective-permute-start(bf16[24,2048]{1,0:T(8,128)(2,1)S(1)} %get-tuple-element.77), channel_id=1, source_target_pairs={{0,4},{2,6},{4,8},{6,10},{8,12},{10,14},{12,16},{14,18},{16,20},{1... | collective-permute-start | bytes 294920 | tf_op jit(solution)/shard_map/ppermute | solution.py:117
  386.4 4.5 collective-permute-start.30
  390.9 22.9 %collective-permute-start.31 = (bf16[24,2048]{1,0:T(8,128)(2,1)S(1)}, bf16[24,2048]{1,0:T(8,128)(2,1)S(1)}, u32[]{:S(2)}, u32[]{:S(2)}) collective-permute-start(bf16[24,2048]{1,0:T(8,128)(2,1)S(1)} %get-tuple-element.74), channel_id=1, source_target_pairs={{0,56},{2,58},{4,60},{6,62},{8,0},{10,2},{12,4},{14,6},{16,8},{18,... | collective-permute-start | bytes 294920 | tf_op jit(solution)/shard_map/ppermute | solution.py:117
  413.9 2.2 collective-permute-start.32
  416.1 10.0 %collective-permute-start.33 = (bf16[24,2048]{1,0:T(8,128)(2,1)S(1)}, bf16[24,2048]{1,0:T(8,128)(2,1)S(1)}, u32[]{:S(2)}, u32[]{:S(2)}) collective-permute-start(bf16[24,2048]{1,0:T(8,128)(2,1)S(1)} %get-tuple-element.72), channel_id=1, source_target_pairs={{0,54},{2,56},{4,58},{6,60},{8,62},{10,0},{12,2},{14,4},{16,6},{18... | collective-permute-start | bytes 294920 | tf_op jit(solution)/shard_map/ppermute | solution.py:117
  426.2 9.3 %collective-permute-start.35 = (bf16[24,2048]{1,0:T(8,128)(2,1)S(1)}, bf16[24,2048]{1,0:T(8,128)(2,1)S(1)}, u32[]{:S(2)}, u32[]{:S(2)}) collective-permute-start(bf16[24,2048]{1,0:T(8,128)(2,1)S(1)} %get-tuple-element.70), channel_id=1, source_target_pairs={{0,52},{2,54},{4,56},{6,58},{8,60},{10,62},{12,0},{14,2},{16,4},{1... | collective-permute-start | bytes 294920 | tf_op jit(solution)/shard_map/ppermute | solution.py:117
  435.5 2.4 collective-permute-start.36
  438.0 4.7 collective-permute-start.37
  442.7 4.6 collective-permute-start.38
  447.3 7.0 %collective-permute-start.39 = (bf16[24,2048]{1,0:T(8,128)(2,1)S(1)}, bf16[24,2048]{1,0:T(8,128)(2,1)S(1)}, u32[]{:S(2)}, u32[]{:S(2)}) collective-permute-start(bf16[24,2048]{1,0:T(8,128)(2,1)S(1)} %get-tuple-element.66), channel_id=1, source_target_pairs={{0,48},{2,50},{4,52},{6,54},{8,56},{10,58},{12,60},{14,62},{16,0},... | collective-permute-start | bytes 294920 | tf_op jit(solution)/shard_map/ppermute | solution.py:117
  454.3 3.4 collective-permute-start.40
  457.7 13.3 %collective-permute-start.41 = (bf16[24,2048]{1,0:T(8,128)(2,1)S(1)}, bf16[24,2048]{1,0:T(8,128)(2,1)S(1)}, u32[]{:S(2)}, u32[]{:S(2)}) collective-permute-start(bf16[24,2048]{1,0:T(8,128)(2,1)S(1)} %get-tuple-element.64), channel_id=1, source_target_pairs={{0,46},{2,48},{4,50},{6,52},{8,54},{10,56},{12,58},{14,60},{16,62}... | collective-permute-start | bytes 294920 | tf_op jit(solution)/shard_map/ppermute | solution.py:117
  471.9 13.8 %collective-permute-start.43 = (bf16[24,2048]{1,0:T(8,128)(2,1)S(1)}, bf16[24,2048]{1,0:T(8,128)(2,1)S(1)}, u32[]{:S(2)}, u32[]{:S(2)}) collective-permute-start(bf16[24,2048]{1,0:T(8,128)(2,1)S(1)} %get-tuple-element.62), channel_id=1, source_target_pairs={{0,44},{2,46},{4,48},{6,50},{8,52},{10,54},{12,56},{14,58},{16,60}... | collective-permute-start | bytes 294920 | tf_op jit(solution)/shard_map/ppermute | solution.py:117
  485.7 12.8 %collective-permute-done.39.refs_15_ = bf16[24,2048]{1,0:T(8,128)(2,1)S(1)} collective-permute-done((bf16[24,2048]{1,0:T(8,128)(2,1)S(1)}, bf16[24,2048]{1,0:T(8,128)(2,1)S(1)}, u32[]{:S(2)}, u32[]{:S(2)}) %collective-permute-start.39) | collective-permute-done | bytes 98336 | tf_op jit(solution)/shard_map/ppermute | solution.py:117
  499.6 19.2 %collective-permute-start.45 = (bf16[24,2048]{1,0:T(8,128)(2,1)S(1)}, bf16[24,2048]{1,0:T(8,128)(2,1)S(1)}, u32[]{:S(2)}, u32[]{:S(2)}) collective-permute-start(bf16[24,2048]{1,0:T(8,128)(2,1)S(1)} %get-tuple-element.60), channel_id=1, source_target_pairs={{0,42},{2,44},{4,46},{6,48},{8,50},{10,52},{12,54},{14,56},{16,58}... | collective-permute-start | bytes 294920 | tf_op jit(solution)/shard_map/ppermute | solution.py:117
  518.9 8.2 %collective-permute-done.43.refs_19_ = bf16[24,2048]{1,0:T(8,128)(2,1)S(1)} collective-permute-done((bf16[24,2048]{1,0:T(8,128)(2,1)S(1)}, bf16[24,2048]{1,0:T(8,128)(2,1)S(1)}, u32[]{:S(2)}, u32[]{:S(2)}) %collective-permute-start.43) | collective-permute-done | bytes 98336 | tf_op jit(solution)/shard_map/ppermute | solution.py:117
  527.1 10.0 %collective-permute-start.27 = (bf16[24,2048]{1,0:T(8,128)(2,1)S(1)}, bf16[24,2048]{1,0:T(8,128)(2,1)S(1)}, u32[]{:S(2)}, u32[]{:S(2)}) collective-permute-start(bf16[24,2048]{1,0:T(8,128)(2,1)S(1)} %get-tuple-element.78), channel_id=1, source_target_pairs={{0,60},{2,62},{4,0},{6,2},{8,4},{10,6},{12,8},{14,10},{16,12},{18,... | collective-permute-start | bytes 294920 | tf_op jit(solution)/shard_map/ppermute | solution.py:117
  537.1 27.2 %collective-permute-start.60 = (bf16[24,2048]{1,0:T(8,128)(2,1)}, bf16[24,2048]{1,0:T(8,128)(2,1)S(1)}, u32[]{:S(2)}, u32[]{:S(2)}) collective-permute-start(bf16[24,2048]{1,0:T(8,128)(2,1)} %get-tuple-element.86), channel_id=1, source_target_pairs={{0,36},{2,38},{4,40},{6,42},{8,44},{10,46},{12,48},{14,50},{16,52}... | collective-permute-start | bytes 294920 | tf_op jit(solution)/shard_map/ppermute | solution.py:117
  564.3 19.2 %collective-permute-start.62 = (bf16[24,2048]{1,0:T(8,128)(2,1)}, bf16[24,2048]{1,0:T(8,128)(2,1)S(1)}, u32[]{:S(2)}, u32[]{:S(2)}) collective-permute-start(bf16[24,2048]{1,0:T(8,128)(2,1)} %get-tuple-element.84), channel_id=1, source_target_pairs={{0,34},{2,36},{4,38},{6,40},{8,42},{10,44},{12,46},{14,48},{16,50}... | collective-permute-start | bytes 294920 | tf_op jit(solution)/shard_map/ppermute | solution.py:117
  584.8 15.1 %collective-permute-start.64 = (bf16[24,2048]{1,0:T(8,128)(2,1)}, bf16[24,2048]{1,0:T(8,128)(2,1)S(1)}, u32[]{:S(2)}, u32[]{:S(2)}) collective-permute-start(bf16[24,2048]{1,0:T(8,128)(2,1)} %get-tuple-element.82), channel_id=1, source_target_pairs={{0,32},{2,34},{4,36},{6,38},{8,40},{10,42},{12,44},{14,46},{16,48}... | collective-permute-start | bytes 294920 | tf_op jit(solution)/shard_map/ppermute | solution.py:117
  600.1 1.9 shard_map.74.refs_2_
  602.0 15.9 %collective-permute-done.62.refs_9_ = bf16[24,2048]{1,0:T(8,128)(2,1)S(1)} collective-permute-done((bf16[24,2048]{1,0:T(8,128)(2,1)}, bf16[24,2048]{1,0:T(8,128)(2,1)S(1)}, u32[]{:S(2)}, u32[]{:S(2)}) %collective-permute-start.62) | collective-permute-done | bytes 98336 | tf_op jit(solution)/shard_map/ppermute | solution.py:117
  618.0 5.7 collective-permute-done.63.refs_10_
  623.7 24.8 %collective-permute-done.64.refs_11_ = bf16[24,2048]{1,0:T(8,128)(2,1)S(1)} collective-permute-done((bf16[24,2048]{1,0:T(8,128)(2,1)}, bf16[24,2048]{1,0:T(8,128)(2,1)S(1)}, u32[]{:S(2)}, u32[]{:S(2)}) %collective-permute-start.64) | collective-permute-done | bytes 98336 | tf_op jit(solution)/shard_map/ppermute | solution.py:117
  648.5 1.9 shard_map.75
  (135 shorter events, 21.7 us)
Async XLA Ops:
  4.1 24.5 %collective-permute-start = (bf16[24,2048]{1,0:T(8,128)(2,1)S(1)}, bf16[24,2048]{1,0:T(8,128)(2,1)S(1)}, u32[]{:S(2)}, u32[]{:S(2)}) collective-permute-start(bf16[24,2048]{1,0:T(8,128)(2,1)S(1)} %get-tuple-element.57), channel_id=1, source_target_pairs={{0,2},{2,4},{4,6},{6,8},{8,10},{10,12},{12,14},{14,16},{16,18},{18... | collective-permute-start | bytes 294920 | tf_op jit(solution)/shard_map/ppermute | solution.py:117
  6.1 27.0 %collective-permute-start.1 = (bf16[24,2048]{1,0:T(8,128)(2,1)S(1)}, bf16[24,2048]{1,0:T(8,128)(2,1)S(1)}, u32[]{:S(2)}, u32[]{:S(2)}) collective-permute-start(bf16[24,2048]{1,0:T(8,128)(2,1)S(1)} %get-tuple-element.56), channel_id=1, source_target_pairs={{0,62},{2,0},{4,2},{6,4},{8,6},{10,8},{12,10},{14,12},{16,14},{18,... | collective-permute-start | bytes 294920 | tf_op jit(solution)/shard_map/ppermute | solution.py:117
  6.1 27.2 %collective-permute-start.2 = (bf16[24,2048]{1,0:T(8,128)(2,1)S(1)}, bf16[24,2048]{1,0:T(8,128)(2,1)S(1)}, u32[]{:S(2)}, u32[]{:S(2)}) collective-permute-start(bf16[24,2048]{1,0:T(8,128)(2,1)S(1)} %get-tuple-element.55), channel_id=1, source_target_pairs={{0,4},{2,6},{4,8},{6,10},{8,12},{10,14},{12,16},{14,18},{16,20},{1... | collective-permute-start | bytes 294920 | tf_op jit(solution)/shard_map/ppermute | solution.py:117
  10.7 28.0 %collective-permute-start.3 = (bf16[24,2048]{1,0:T(8,128)(2,1)S(1)}, bf16[24,2048]{1,0:T(8,128)(2,1)S(1)}, u32[]{:S(2)}, u32[]{:S(2)}) collective-permute-start(bf16[24,2048]{1,0:T(8,128)(2,1)S(1)} %get-tuple-element.54), channel_id=1, source_target_pairs={{0,60},{2,62},{4,0},{6,2},{8,4},{10,6},{12,8},{14,10},{16,12},{18,... | collective-permute-start | bytes 294920 | tf_op jit(solution)/shard_map/ppermute | solution.py:117
  28.6 16.6 %collective-permute-start.5 = (bf16[24,2048]{1,0:T(8,128)(2,1)S(1)}, bf16[24,2048]{1,0:T(8,128)(2,1)S(1)}, u32[]{:S(2)}, u32[]{:S(2)}) collective-permute-start(bf16[24,2048]{1,0:T(8,128)(2,1)S(1)} %get-tuple-element.52), channel_id=1, source_target_pairs={{0,58},{2,60},{4,62},{6,0},{8,2},{10,4},{12,6},{14,8},{16,10},{18,... | collective-permute-start | bytes 294920 | tf_op jit(solution)/shard_map/ppermute | solution.py:117
  33.1 14.6 %collective-permute-start.6 = (bf16[24,2048]{1,0:T(8,128)(2,1)S(1)}, bf16[24,2048]{1,0:T(8,128)(2,1)S(1)}, u32[]{:S(2)}, u32[]{:S(2)}) collective-permute-start(bf16[24,2048]{1,0:T(8,128)(2,1)S(1)} %get-tuple-element.51), channel_id=1, source_target_pairs={{0,8},{2,10},{4,12},{6,14},{8,16},{10,18},{12,20},{14,22},{16,24},... | collective-permute-start | bytes 294920 | tf_op jit(solution)/shard_map/ppermute | solution.py:117
  33.2 22.3 %collective-permute-start.7 = (bf16[24,2048]{1,0:T(8,128)(2,1)S(1)}, bf16[24,2048]{1,0:T(8,128)(2,1)S(1)}, u32[]{:S(2)}, u32[]{:S(2)}) collective-permute-start(bf16[24,2048]{1,0:T(8,128)(2,1)S(1)} %get-tuple-element.50), channel_id=1, source_target_pairs={{0,56},{2,58},{4,60},{6,62},{8,0},{10,2},{12,4},{14,6},{16,8},{18,... | collective-permute-start | bytes 294920 | tf_op jit(solution)/shard_map/ppermute | solution.py:117
  38.7 21.1 %collective-permute-start.8 = (bf16[24,2048]{1,0:T(8,128)(2,1)S(1)}, bf16[24,2048]{1,0:T(8,128)(2,1)S(1)}, u32[]{:S(2)}, u32[]{:S(2)}) collective-permute-start(bf16[24,2048]{1,0:T(8,128)(2,1)S(1)} %get-tuple-element.49), channel_id=1, source_target_pairs={{0,10},{2,12},{4,14},{6,16},{8,18},{10,20},{12,22},{14,24},{16,26}... | collective-permute-start | bytes 294920 | tf_op jit(solution)/shard_map/ppermute | solution.py:117
  38.8 26.6 %collective-permute-start.9 = (bf16[24,2048]{1,0:T(8,128)(2,1)S(1)}, bf16[24,2048]{1,0:T(8,128)(2,1)S(1)}, u32[]{:S(2)}, u32[]{:S(2)}) collective-permute-start(bf16[24,2048]{1,0:T(8,128)(2,1)S(1)} %get-tuple-element.48), channel_id=1, source_target_pairs={{0,54},{2,56},{4,58},{6,60},{8,62},{10,0},{12,2},{14,4},{16,6},{18... | collective-permute-start | bytes 294920 | tf_op jit(solution)/shard_map/ppermute | solution.py:117
  45.2 26.4 %collective-permute-start.10 = (bf16[24,2048]{1,0:T(8,128)(2,1)S(1)}, bf16[24,2048]{1,0:T(8,128)(2,1)S(1)}, u32[]{:S(2)}, u32[]{:S(2)}) collective-permute-start(bf16[24,2048]{1,0:T(8,128)(2,1)S(1)} %get-tuple-element.47), channel_id=1, source_target_pairs={{0,12},{2,14},{4,16},{6,18},{8,20},{10,22},{12,24},{14,26},{16,28}... | collective-permute-start | bytes 294920 | tf_op jit(solution)/shard_map/ppermute | solution.py:117
  47.7 28.2 %collective-permute-start.11 = (bf16[24,2048]{1,0:T(8,128)(2,1)S(1)}, bf16[24,2048]{1,0:T(8,128)(2,1)S(1)}, u32[]{:S(2)}, u32[]{:S(2)}) collective-permute-start(bf16[24,2048]{1,0:T(8,128)(2,1)S(1)} %get-tuple-element.46), channel_id=1, source_target_pairs={{0,52},{2,54},{4,56},{6,58},{8,60},{10,62},{12,0},{14,2},{16,4},{1... | collective-permute-start | bytes 294920 | tf_op jit(solution)/shard_map/ppermute | solution.py:117
  55.5 40.7 %collective-permute-start.12 = (bf16[24,2048]{1,0:T(8,128)(2,1)S(1)}, bf16[24,2048]{1,0:T(8,128)(2,1)S(1)}, u32[]{:S(2)}, u32[]{:S(2)}) collective-permute-start(bf16[24,2048]{1,0:T(8,128)(2,1)S(1)} %get-tuple-element.45), channel_id=1, source_target_pairs={{0,14},{2,16},{4,18},{6,20},{8,22},{10,24},{12,26},{14,28},{16,30}... | collective-permute-start | bytes 294920 | tf_op jit(solution)/shard_map/ppermute | solution.py:117
  59.7 37.8 %collective-permute-start.13 = (bf16[24,2048]{1,0:T(8,128)(2,1)S(1)}, bf16[24,2048]{1,0:T(8,128)(2,1)S(1)}, u32[]{:S(2)}, u32[]{:S(2)}) collective-permute-start(bf16[24,2048]{1,0:T(8,128)(2,1)S(1)} %get-tuple-element.44), channel_id=1, source_target_pairs={{0,50},{2,52},{4,54},{6,56},{8,58},{10,60},{12,62},{14,0},{16,2},{... | collective-permute-start | bytes 294920 | tf_op jit(solution)/shard_map/ppermute | solution.py:117
  65.4 32.3 %collective-permute-start.14 = (bf16[24,2048]{1,0:T(8,128)(2,1)S(1)}, bf16[24,2048]{1,0:T(8,128)(2,1)S(1)}, u32[]{:S(2)}, u32[]{:S(2)}) collective-permute-start(bf16[24,2048]{1,0:T(8,128)(2,1)S(1)} %get-tuple-element.43), channel_id=1, source_target_pairs={{0,16},{2,18},{4,20},{6,22},{8,24},{10,26},{12,28},{14,30},{16,32}... | collective-permute-start | bytes 294920 | tf_op jit(solution)/shard_map/ppermute | solution.py:117
  71.6 29.3 %collective-permute-start.15 = (bf16[24,2048]{1,0:T(8,128)(2,1)S(1)}, bf16[24,2048]{1,0:T(8,128)(2,1)S(1)}, u32[]{:S(2)}, u32[]{:S(2)}) collective-permute-start(bf16[24,2048]{1,0:T(8,128)(2,1)S(1)} %get-tuple-element.42), channel_id=1, source_target_pairs={{0,48},{2,50},{4,52},{6,54},{8,56},{10,58},{12,60},{14,62},{16,0},... | collective-permute-start | bytes 294920 | tf_op jit(solution)/shard_map/ppermute | solution.py:117
  75.9 49.1 %collective-permute-start.16 = (bf16[24,2048]{1,0:T(8,128)(2,1)S(1)}, bf16[24,2048]{1,0:T(8,128)(2,1)S(1)}, u32[]{:S(2)}, u32[]{:S(2)}) collective-permute-start(bf16[24,2048]{1,0:T(8,128)(2,1)S(1)} %get-tuple-element.41), channel_id=1, source_target_pairs={{0,18},{2,20},{4,22},{6,24},{8,26},{10,28},{12,30},{14,32},{16,34}... | collective-permute-start | bytes 294920 | tf_op jit(solution)/shard_map/ppermute | solution.py:117
  96.2 121.8 %collective-permute-start.23 = (bf16[2048,512]{1,0:T(8,128)(2,1)S(1)}, bf16[2048,512]{1,0:T(8,128)(2,1)S(1)}, u32[]{:S(2)}, u32[]{:S(2)}) collective-permute-start(bf16[2048,512]{1,0:T(8,128)(2,1)S(1)} %bitcast.16), channel_id=1, source_target_pairs={{0,1},{1,0},{2,3},{3,2},{4,5},{5,4},{6,7},{7,6},{8,9},{9,8},{10,11... | collective-permute-start | bytes 6291464 | tf_op jit(solution)/shard_map/ppermute | solution.py:112
  97.6 27.4 %collective-permute-start.17 = (bf16[24,2048]{1,0:T(8,128)(2,1)S(1)}, bf16[24,2048]{1,0:T(8,128)(2,1)S(1)}, u32[]{:S(2)}, u32[]{:S(2)}) collective-permute-start(bf16[24,2048]{1,0:T(8,128)(2,1)S(1)} %get-tuple-element.40), channel_id=1, source_target_pairs={{0,46},{2,48},{4,50},{6,52},{8,54},{10,56},{12,58},{14,60},{16,62}... | collective-permute-start | bytes 294920 | tf_op jit(solution)/shard_map/ppermute | solution.py:117
  97.8 156.4 %collective-permute-start.22 = (bf16[2048,512]{1,0:T(8,128)(2,1)S(1)}, bf16[2048,512]{1,0:T(8,128)(2,1)S(1)}, u32[]{:S(2)}, u32[]{:S(2)}) collective-permute-start(bf16[2048,512]{1,0:T(8,128)(2,1)S(1)} %bitcast.23), channel_id=1, source_target_pairs={{0,1},{1,0},{2,3},{3,2},{4,5},{5,4},{6,7},{7,6},{8,9},{9,8},{10,11... | collective-permute-start | bytes 6291464 | tf_op jit(solution)/shard_map/ppermute | solution.py:112
  101.0 163.4 %collective-permute-start.24 = (bf16[512,2048]{1,0:T(8,128)(2,1)S(1)}, bf16[512,2048]{1,0:T(8,128)(2,1)S(1)}, u32[]{:S(2)}, u32[]{:S(2)}) collective-permute-start(bf16[512,2048]{1,0:T(8,128)(2,1)S(1)} %bitcast.20), channel_id=1, source_target_pairs={{0,1},{1,0},{2,3},{3,2},{4,5},{5,4},{6,7},{7,6},{8,9},{9,8},{10,11... | collective-permute-start | bytes 6291464 | tf_op jit(solution)/shard_map/ppermute | solution.py:112
  125.0 25.9 %collective-permute-start.18 = (bf16[24,2048]{1,0:T(8,128)(2,1)S(1)}, bf16[24,2048]{1,0:T(8,128)(2,1)S(1)}, u32[]{:S(2)}, u32[]{:S(2)}) collective-permute-start(bf16[24,2048]{1,0:T(8,128)(2,1)S(1)} %get-tuple-element.39), channel_id=1, source_target_pairs={{0,20},{2,22},{4,24},{6,26},{8,28},{10,30},{12,32},{14,34},{16,36}... | collective-permute-start | bytes 294920 | tf_op jit(solution)/shard_map/ppermute | solution.py:117
  125.0 27.7 %collective-permute-start.19 = (bf16[24,2048]{1,0:T(8,128)(2,1)S(1)}, bf16[24,2048]{1,0:T(8,128)(2,1)S(1)}, u32[]{:S(2)}, u32[]{:S(2)}) collective-permute-start(bf16[24,2048]{1,0:T(8,128)(2,1)S(1)} %get-tuple-element.38), channel_id=1, source_target_pairs={{0,44},{2,46},{4,48},{6,50},{8,52},{10,54},{12,56},{14,58},{16,60}... | collective-permute-start | bytes 294920 | tf_op jit(solution)/shard_map/ppermute | solution.py:117
  150.8 30.3 %collective-permute-start.20 = (bf16[24,2048]{1,0:T(8,128)(2,1)S(1)}, bf16[24,2048]{1,0:T(8,128)(2,1)S(1)}, u32[]{:S(2)}, u32[]{:S(2)}) collective-permute-start(bf16[24,2048]{1,0:T(8,128)(2,1)S(1)} %get-tuple-element.37), channel_id=1, source_target_pairs={{0,22},{2,24},{4,26},{6,28},{8,30},{10,32},{12,34},{14,36},{16,38}... | collective-permute-start | bytes 294920 | tf_op jit(solution)/shard_map/ppermute | solution.py:117
  152.7 28.6 %collective-permute-start.21 = (bf16[24,2048]{1,0:T(8,128)(2,1)S(1)}, bf16[24,2048]{1,0:T(8,128)(2,1)S(1)}, u32[]{:S(2)}, u32[]{:S(2)}) collective-permute-start(bf16[24,2048]{1,0:T(8,128)(2,1)S(1)} %get-tuple-element.36), channel_id=1, source_target_pairs={{0,42},{2,44},{4,46},{6,48},{8,50},{10,52},{12,54},{14,56},{16,58}... | collective-permute-start | bytes 294920 | tf_op jit(solution)/shard_map/ppermute | solution.py:117
  181.1 18.9 %collective-permute-start.47 = (bf16[24,2048]{1,0:T(8,128)(2,1)S(1)}, bf16[24,2048]{1,0:T(8,128)(2,1)S(1)}, u32[]{:S(2)}, u32[]{:S(2)}) collective-permute-start(bf16[24,2048]{1,0:T(8,128)(2,1)S(1)} %get-tuple-element.35), channel_id=1, source_target_pairs={{0,24},{2,26},{4,28},{6,30},{8,32},{10,34},{12,36},{14,38},{16,40}... | collective-permute-start | bytes 294920 | tf_op jit(solution)/shard_map/ppermute | solution.py:117
  181.3 46.2 %collective-permute-start.48 = (bf16[24,2048]{1,0:T(8,128)(2,1)S(1)}, bf16[24,2048]{1,0:T(8,128)(2,1)S(1)}, u32[]{:S(2)}, u32[]{:S(2)}) collective-permute-start(bf16[24,2048]{1,0:T(8,128)(2,1)S(1)} %get-tuple-element.34), channel_id=1, source_target_pairs={{0,40},{2,42},{4,44},{6,46},{8,48},{10,50},{12,52},{14,54},{16,56}... | collective-permute-start | bytes 294920 | tf_op jit(solution)/shard_map/ppermute | solution.py:117
  200.0 41.4 %collective-permute-start.49 = (bf16[24,2048]{1,0:T(8,128)(2,1)S(1)}, bf16[24,2048]{1,0:T(8,128)(2,1)S(1)}, u32[]{:S(2)}, u32[]{:S(2)}) collective-permute-start(bf16[24,2048]{1,0:T(8,128)(2,1)S(1)} %get-tuple-element.33), channel_id=1, source_target_pairs={{0,26},{2,28},{4,30},{6,32},{8,34},{10,36},{12,38},{14,40},{16,42}... | collective-permute-start | bytes 294920 | tf_op jit(solution)/shard_map/ppermute | solution.py:117
  218.1 27.4 %collective-permute-start.50 = (bf16[24,2048]{1,0:T(8,128)(2,1)S(1)}, bf16[24,2048]{1,0:T(8,128)(2,1)S(1)}, u32[]{:S(2)}, u32[]{:S(2)}) collective-permute-start(bf16[24,2048]{1,0:T(8,128)(2,1)S(1)} %get-tuple-element.32), channel_id=1, source_target_pairs={{0,38},{2,40},{4,42},{6,44},{8,46},{10,48},{12,50},{14,52},{16,54}... | collective-permute-start | bytes 294920 | tf_op jit(solution)/shard_map/ppermute | solution.py:117
  227.5 78.1 %collective-permute-start.51 = (bf16[24,2048]{1,0:T(8,128)(2,1)}, bf16[24,2048]{1,0:T(8,128)(2,1)S(1)}, u32[]{:S(2)}, u32[]{:S(2)}) collective-permute-start(bf16[24,2048]{1,0:T(8,128)(2,1)} %get-tuple-element.31), channel_id=1, source_target_pairs={{0,28},{2,30},{4,32},{6,34},{8,36},{10,38},{12,40},{14,42},{16,44}... | collective-permute-start | bytes 294920 | tf_op jit(solution)/shard_map/ppermute | solution.py:117
  241.4 64.1 %collective-permute-start.52 = (bf16[24,2048]{1,0:T(8,128)(2,1)S(1)}, bf16[24,2048]{1,0:T(8,128)(2,1)S(1)}, u32[]{:S(2)}, u32[]{:S(2)}) collective-permute-start(bf16[24,2048]{1,0:T(8,128)(2,1)S(1)} %get-tuple-element.30), channel_id=1, source_target_pairs={{0,36},{2,38},{4,40},{6,42},{8,44},{10,46},{12,48},{14,50},{16,52}... | collective-permute-start | bytes 294920 | tf_op jit(solution)/shard_map/ppermute | solution.py:117
  245.5 60.1 %collective-permute-start.53 = (bf16[24,2048]{1,0:T(8,128)(2,1)S(1)}, bf16[24,2048]{1,0:T(8,128)(2,1)S(1)}, u32[]{:S(2)}, u32[]{:S(2)}) collective-permute-start(bf16[24,2048]{1,0:T(8,128)(2,1)S(1)} %get-tuple-element.29), channel_id=1, source_target_pairs={{0,30},{2,32},{4,34},{6,36},{8,38},{10,40},{12,42},{14,44},{16,46}... | collective-permute-start | bytes 294920 | tf_op jit(solution)/shard_map/ppermute | solution.py:117
  254.1 69.0 %collective-permute-start.54 = (bf16[24,2048]{1,0:T(8,128)(2,1)S(1)}, bf16[24,2048]{1,0:T(8,128)(2,1)S(1)}, u32[]{:S(2)}, u32[]{:S(2)}) collective-permute-start(bf16[24,2048]{1,0:T(8,128)(2,1)S(1)} %get-tuple-element.28), channel_id=1, source_target_pairs={{0,34},{2,36},{4,38},{6,40},{8,42},{10,44},{12,46},{14,48},{16,50}... | collective-permute-start | bytes 294920 | tf_op jit(solution)/shard_map/ppermute | solution.py:117
  265.8 57.4 %collective-permute-start.55 = (bf16[24,2048]{1,0:T(8,128)(2,1)S(1)}, bf16[24,2048]{1,0:T(8,128)(2,1)S(1)}, u32[]{:S(2)}, u32[]{:S(2)}) collective-permute-start(bf16[24,2048]{1,0:T(8,128)(2,1)S(1)} %get-tuple-element.27), channel_id=1, source_target_pairs={{0,32},{2,34},{4,36},{6,38},{8,40},{10,42},{12,44},{14,46},{16,48}... | collective-permute-start | bytes 294920 | tf_op jit(solution)/shard_map/ppermute | solution.py:117
  340.3 46.1 %collective-permute-start.56 = (bf16[24,2048]{1,0:T(8,128)(2,1)S(1)}, bf16[24,2048]{1,0:T(8,128)(2,1)S(1)}, u32[]{:S(2)}, u32[]{:S(2)}) collective-permute-start(bf16[24,2048]{1,0:T(8,128)(2,1)S(1)} %get-tuple-element.90), channel_id=1, source_target_pairs={{0,40},{2,42},{4,44},{6,46},{8,48},{10,50},{12,52},{14,54},{16,56}... | collective-permute-start | bytes 294920 | tf_op jit(solution)/shard_map/ppermute | solution.py:117
  344.7 41.7 %collective-permute-start.57 = (bf16[24,2048]{1,0:T(8,128)(2,1)S(1)}, bf16[24,2048]{1,0:T(8,128)(2,1)S(1)}, u32[]{:S(2)}, u32[]{:S(2)}) collective-permute-start(bf16[24,2048]{1,0:T(8,128)(2,1)S(1)} %get-tuple-element.89), channel_id=1, source_target_pairs={{0,24},{2,26},{4,28},{6,30},{8,32},{10,34},{12,36},{14,38},{16,40}... | collective-permute-start | bytes 294920 | tf_op jit(solution)/shard_map/ppermute | solution.py:117
  358.3 32.6 %collective-permute-start.58 = (bf16[24,2048]{1,0:T(8,128)(2,1)S(1)}, bf16[24,2048]{1,0:T(8,128)(2,1)S(1)}, u32[]{:S(2)}, u32[]{:S(2)}) collective-permute-start(bf16[24,2048]{1,0:T(8,128)(2,1)S(1)} %get-tuple-element.88), channel_id=1, source_target_pairs={{0,38},{2,40},{4,42},{6,44},{8,46},{10,48},{12,50},{14,52},{16,54}... | collective-permute-start | bytes 294920 | tf_op jit(solution)/shard_map/ppermute | solution.py:117
  363.5 50.4 %collective-permute-start.59 = (bf16[24,2048]{1,0:T(8,128)(2,1)S(1)}, bf16[24,2048]{1,0:T(8,128)(2,1)S(1)}, u32[]{:S(2)}, u32[]{:S(2)}) collective-permute-start(bf16[24,2048]{1,0:T(8,128)(2,1)S(1)} %get-tuple-element.87), channel_id=1, source_target_pairs={{0,26},{2,28},{4,30},{6,32},{8,34},{10,36},{12,38},{14,40},{16,42}... | collective-permute-start | bytes 294920 | tf_op jit(solution)/shard_map/ppermute | solution.py:117
  374.3 41.8 %collective-permute-start.28 = (bf16[24,2048]{1,0:T(8,128)(2,1)S(1)}, bf16[24,2048]{1,0:T(8,128)(2,1)S(1)}, u32[]{:S(2)}, u32[]{:S(2)}) collective-permute-start(bf16[24,2048]{1,0:T(8,128)(2,1)S(1)} %get-tuple-element.77), channel_id=1, source_target_pairs={{0,4},{2,6},{4,8},{6,10},{8,12},{10,14},{12,16},{14,18},{16,20},{1... | collective-permute-start | bytes 294920 | tf_op jit(solution)/shard_map/ppermute | solution.py:117
  386.4 39.7 %collective-permute-start.29 = (bf16[24,2048]{1,0:T(8,128)(2,1)S(1)}, bf16[24,2048]{1,0:T(8,128)(2,1)S(1)}, u32[]{:S(2)}, u32[]{:S(2)}) collective-permute-start(bf16[24,2048]{1,0:T(8,128)(2,1)S(1)} %get-tuple-element.76), channel_id=1, source_target_pairs={{0,58},{2,60},{4,62},{6,0},{8,2},{10,4},{12,6},{14,8},{16,10},{18,... | collective-permute-start | bytes 294920 | tf_op jit(solution)/shard_map/ppermute | solution.py:117
  386.4 39.8 %collective-permute-start.30 = (bf16[24,2048]{1,0:T(8,128)(2,1)S(1)}, bf16[24,2048]{1,0:T(8,128)(2,1)S(1)}, u32[]{:S(2)}, u32[]{:S(2)}) collective-permute-start(bf16[24,2048]{1,0:T(8,128)(2,1)S(1)} %get-tuple-element.75), channel_id=1, source_target_pairs={{0,6},{2,8},{4,10},{6,12},{8,14},{10,16},{12,18},{14,20},{16,22},{... | collective-permute-start | bytes 294920 | tf_op jit(solution)/shard_map/ppermute | solution.py:117
  390.9 44.6 %collective-permute-start.31 = (bf16[24,2048]{1,0:T(8,128)(2,1)S(1)}, bf16[24,2048]{1,0:T(8,128)(2,1)S(1)}, u32[]{:S(2)}, u32[]{:S(2)}) collective-permute-start(bf16[24,2048]{1,0:T(8,128)(2,1)S(1)} %get-tuple-element.74), channel_id=1, source_target_pairs={{0,56},{2,58},{4,60},{6,62},{8,0},{10,2},{12,4},{14,6},{16,8},{18,... | collective-permute-start | bytes 294920 | tf_op jit(solution)/shard_map/ppermute | solution.py:117
  413.9 24.1 %collective-permute-start.32 = (bf16[24,2048]{1,0:T(8,128)(2,1)S(1)}, bf16[24,2048]{1,0:T(8,128)(2,1)S(1)}, u32[]{:S(2)}, u32[]{:S(2)}) collective-permute-start(bf16[24,2048]{1,0:T(8,128)(2,1)S(1)} %get-tuple-element.73), channel_id=1, source_target_pairs={{0,8},{2,10},{4,12},{6,14},{8,16},{10,18},{12,20},{14,22},{16,24},... | collective-permute-start | bytes 294920 | tf_op jit(solution)/shard_map/ppermute | solution.py:117
  416.1 26.6 %collective-permute-start.33 = (bf16[24,2048]{1,0:T(8,128)(2,1)S(1)}, bf16[24,2048]{1,0:T(8,128)(2,1)S(1)}, u32[]{:S(2)}, u32[]{:S(2)}) collective-permute-start(bf16[24,2048]{1,0:T(8,128)(2,1)S(1)} %get-tuple-element.72), channel_id=1, source_target_pairs={{0,54},{2,56},{4,58},{6,60},{8,62},{10,0},{12,2},{14,4},{16,6},{18... | collective-permute-start | bytes 294920 | tf_op jit(solution)/shard_map/ppermute | solution.py:117
  426.1 21.1 %collective-permute-start.34 = (bf16[24,2048]{1,0:T(8,128)(2,1)S(1)}, bf16[24,2048]{1,0:T(8,128)(2,1)S(1)}, u32[]{:S(2)}, u32[]{:S(2)}) collective-permute-start(bf16[24,2048]{1,0:T(8,128)(2,1)S(1)} %get-tuple-element.71), channel_id=1, source_target_pairs={{0,10},{2,12},{4,14},{6,16},{8,18},{10,20},{12,22},{14,24},{16,26}... | collective-permute-start | bytes 294920 | tf_op jit(solution)/shard_map/ppermute | solution.py:117
  426.2 28.0 %collective-permute-start.35 = (bf16[24,2048]{1,0:T(8,128)(2,1)S(1)}, bf16[24,2048]{1,0:T(8,128)(2,1)S(1)}, u32[]{:S(2)}, u32[]{:S(2)}) collective-permute-start(bf16[24,2048]{1,0:T(8,128)(2,1)S(1)} %get-tuple-element.70), channel_id=1, source_target_pairs={{0,52},{2,54},{4,56},{6,58},{8,60},{10,62},{12,0},{14,2},{16,4},{1... | collective-permute-start | bytes 294920 | tf_op jit(solution)/shard_map/ppermute | solution.py:117
  435.5 22.1 %collective-permute-start.36 = (bf16[24,2048]{1,0:T(8,128)(2,1)S(1)}, bf16[24,2048]{1,0:T(8,128)(2,1)S(1)}, u32[]{:S(2)}, u32[]{:S(2)}) collective-permute-start(bf16[24,2048]{1,0:T(8,128)(2,1)S(1)} %get-tuple-element.69), channel_id=1, source_target_pairs={{0,12},{2,14},{4,16},{6,18},{8,20},{10,22},{12,24},{14,26},{16,28}... | collective-permute-start | bytes 294920 | tf_op jit(solution)/shard_map/ppermute | solution.py:117
  438.0 33.9 %collective-permute-start.37 = (bf16[24,2048]{1,0:T(8,128)(2,1)S(1)}, bf16[24,2048]{1,0:T(8,128)(2,1)S(1)}, u32[]{:S(2)}, u32[]{:S(2)}) collective-permute-start(bf16[24,2048]{1,0:T(8,128)(2,1)S(1)} %get-tuple-element.68), channel_id=1, source_target_pairs={{0,50},{2,52},{4,54},{6,56},{8,58},{10,60},{12,62},{14,0},{16,2},{... | collective-permute-start | bytes 294920 | tf_op jit(solution)/shard_map/ppermute | solution.py:117
  442.7 29.2 %collective-permute-start.38 = (bf16[24,2048]{1,0:T(8,128)(2,1)S(1)}, bf16[24,2048]{1,0:T(8,128)(2,1)S(1)}, u32[]{:S(2)}, u32[]{:S(2)}) collective-permute-start(bf16[24,2048]{1,0:T(8,128)(2,1)S(1)} %get-tuple-element.67), channel_id=1, source_target_pairs={{0,14},{2,16},{4,18},{6,20},{8,22},{10,24},{12,26},{14,28},{16,30}... | collective-permute-start | bytes 294920 | tf_op jit(solution)/shard_map/ppermute | solution.py:117
  447.3 51.2 %collective-permute-start.39 = (bf16[24,2048]{1,0:T(8,128)(2,1)S(1)}, bf16[24,2048]{1,0:T(8,128)(2,1)S(1)}, u32[]{:S(2)}, u32[]{:S(2)}) collective-permute-start(bf16[24,2048]{1,0:T(8,128)(2,1)S(1)} %get-tuple-element.66), channel_id=1, source_target_pairs={{0,48},{2,50},{4,52},{6,54},{8,56},{10,58},{12,60},{14,62},{16,0},... | collective-permute-start | bytes 294920 | tf_op jit(solution)/shard_map/ppermute | solution.py:117
  454.3 45.3 %collective-permute-start.40 = (bf16[24,2048]{1,0:T(8,128)(2,1)S(1)}, bf16[24,2048]{1,0:T(8,128)(2,1)S(1)}, u32[]{:S(2)}, u32[]{:S(2)}) collective-permute-start(bf16[24,2048]{1,0:T(8,128)(2,1)S(1)} %get-tuple-element.65), channel_id=1, source_target_pairs={{0,16},{2,18},{4,20},{6,22},{8,24},{10,26},{12,28},{14,30},{16,32}... | collective-permute-start | bytes 294920 | tf_op jit(solution)/shard_map/ppermute | solution.py:117
  457.7 61.1 %collective-permute-start.41 = (bf16[24,2048]{1,0:T(8,128)(2,1)S(1)}, bf16[24,2048]{1,0:T(8,128)(2,1)S(1)}, u32[]{:S(2)}, u32[]{:S(2)}) collective-permute-start(bf16[24,2048]{1,0:T(8,128)(2,1)S(1)} %get-tuple-element.64), channel_id=1, source_target_pairs={{0,46},{2,48},{4,50},{6,52},{8,54},{10,56},{12,58},{14,60},{16,62}... | collective-permute-start | bytes 294920 | tf_op jit(solution)/shard_map/ppermute | solution.py:117
  471.9 46.9 %collective-permute-start.42 = (bf16[24,2048]{1,0:T(8,128)(2,1)S(1)}, bf16[24,2048]{1,0:T(8,128)(2,1)S(1)}, u32[]{:S(2)}, u32[]{:S(2)}) collective-permute-start(bf16[24,2048]{1,0:T(8,128)(2,1)S(1)} %get-tuple-element.63), channel_id=1, source_target_pairs={{0,18},{2,20},{4,22},{6,24},{8,26},{10,28},{12,30},{14,32},{16,34}... | collective-permute-start | bytes 294920 | tf_op jit(solution)/shard_map/ppermute | solution.py:117
  471.9 55.2 %collective-permute-start.43 = (bf16[24,2048]{1,0:T(8,128)(2,1)S(1)}, bf16[24,2048]{1,0:T(8,128)(2,1)S(1)}, u32[]{:S(2)}, u32[]{:S(2)}) collective-permute-start(bf16[24,2048]{1,0:T(8,128)(2,1)S(1)} %get-tuple-element.62), channel_id=1, source_target_pairs={{0,44},{2,46},{4,48},{6,50},{8,52},{10,54},{12,56},{14,58},{16,60}... | collective-permute-start | bytes 294920 | tf_op jit(solution)/shard_map/ppermute | solution.py:117
  498.5 28.6 %collective-permute-start.44 = (bf16[24,2048]{1,0:T(8,128)(2,1)S(1)}, bf16[24,2048]{1,0:T(8,128)(2,1)S(1)}, u32[]{:S(2)}, u32[]{:S(2)}) collective-permute-start(bf16[24,2048]{1,0:T(8,128)(2,1)S(1)} %get-tuple-element.61), channel_id=1, source_target_pairs={{0,20},{2,22},{4,24},{6,26},{8,28},{10,30},{12,32},{14,34},{16,36}... | collective-permute-start | bytes 294920 | tf_op jit(solution)/shard_map/ppermute | solution.py:117
  499.6 37.5 %collective-permute-start.45 = (bf16[24,2048]{1,0:T(8,128)(2,1)S(1)}, bf16[24,2048]{1,0:T(8,128)(2,1)S(1)}, u32[]{:S(2)}, u32[]{:S(2)}) collective-permute-start(bf16[24,2048]{1,0:T(8,128)(2,1)S(1)} %get-tuple-element.60), channel_id=1, source_target_pairs={{0,42},{2,44},{4,46},{6,48},{8,50},{10,52},{12,54},{14,56},{16,58}... | collective-permute-start | bytes 294920 | tf_op jit(solution)/shard_map/ppermute | solution.py:117
  518.8 45.5 %collective-permute-start.46 = (bf16[24,2048]{1,0:T(8,128)(2,1)S(1)}, bf16[24,2048]{1,0:T(8,128)(2,1)S(1)}, u32[]{:S(2)}, u32[]{:S(2)}) collective-permute-start(bf16[24,2048]{1,0:T(8,128)(2,1)S(1)} %get-tuple-element.59), channel_id=1, source_target_pairs={{0,22},{2,24},{4,26},{6,28},{8,30},{10,32},{12,34},{14,36},{16,38}... | collective-permute-start | bytes 294920 | tf_op jit(solution)/shard_map/ppermute | solution.py:117
  518.8 45.5 %collective-permute-start.25 = (bf16[24,2048]{1,0:T(8,128)(2,1)S(1)}, bf16[24,2048]{1,0:T(8,128)(2,1)S(1)}, u32[]{:S(2)}, u32[]{:S(2)}) collective-permute-start(bf16[24,2048]{1,0:T(8,128)(2,1)S(1)} %get-tuple-element.80), channel_id=1, source_target_pairs={{0,62},{2,0},{4,2},{6,4},{8,6},{10,8},{12,10},{14,12},{16,14},{18,... | collective-permute-start | bytes 294920 | tf_op jit(solution)/shard_map/ppermute | solution.py:117
  527.1 56.4 %collective-permute-start.26 = (bf16[24,2048]{1,0:T(8,128)(2,1)S(1)}, bf16[24,2048]{1,0:T(8,128)(2,1)S(1)}, u32[]{:S(2)}, u32[]{:S(2)}) collective-permute-start(bf16[24,2048]{1,0:T(8,128)(2,1)S(1)} %get-tuple-element.79), channel_id=1, source_target_pairs={{0,2},{2,4},{4,6},{6,8},{8,10},{10,12},{12,14},{14,16},{16,18},{18... | collective-permute-start | bytes 294920 | tf_op jit(solution)/shard_map/ppermute | solution.py:117
  527.1 57.6 %collective-permute-start.27 = (bf16[24,2048]{1,0:T(8,128)(2,1)S(1)}, bf16[24,2048]{1,0:T(8,128)(2,1)S(1)}, u32[]{:S(2)}, u32[]{:S(2)}) collective-permute-start(bf16[24,2048]{1,0:T(8,128)(2,1)S(1)} %get-tuple-element.78), channel_id=1, source_target_pairs={{0,60},{2,62},{4,0},{6,2},{8,4},{10,6},{12,8},{14,10},{16,12},{18,... | collective-permute-start | bytes 294920 | tf_op jit(solution)/shard_map/ppermute | solution.py:117
  537.1 64.9 %collective-permute-start.60 = (bf16[24,2048]{1,0:T(8,128)(2,1)}, bf16[24,2048]{1,0:T(8,128)(2,1)S(1)}, u32[]{:S(2)}, u32[]{:S(2)}) collective-permute-start(bf16[24,2048]{1,0:T(8,128)(2,1)} %get-tuple-element.86), channel_id=1, source_target_pairs={{0,36},{2,38},{4,40},{6,42},{8,44},{10,46},{12,48},{14,50},{16,52}... | collective-permute-start | bytes 294920 | tf_op jit(solution)/shard_map/ppermute | solution.py:117
  564.3 37.7 %collective-permute-start.61 = (bf16[24,2048]{1,0:T(8,128)(2,1)}, bf16[24,2048]{1,0:T(8,128)(2,1)S(1)}, u32[]{:S(2)}, u32[]{:S(2)}) collective-permute-start(bf16[24,2048]{1,0:T(8,128)(2,1)} %get-tuple-element.85), channel_id=1, source_target_pairs={{0,28},{2,30},{4,32},{6,34},{8,36},{10,38},{12,40},{14,42},{16,44}... | collective-permute-start | bytes 294920 | tf_op jit(solution)/shard_map/ppermute | solution.py:117
  564.3 53.7 %collective-permute-start.62 = (bf16[24,2048]{1,0:T(8,128)(2,1)}, bf16[24,2048]{1,0:T(8,128)(2,1)S(1)}, u32[]{:S(2)}, u32[]{:S(2)}) collective-permute-start(bf16[24,2048]{1,0:T(8,128)(2,1)} %get-tuple-element.84), channel_id=1, source_target_pairs={{0,34},{2,36},{4,38},{6,40},{8,42},{10,44},{12,46},{14,48},{16,50}... | collective-permute-start | bytes 294920 | tf_op jit(solution)/shard_map/ppermute | solution.py:117
  583.5 40.2 %collective-permute-start.63 = (bf16[24,2048]{1,0:T(8,128)(2,1)}, bf16[24,2048]{1,0:T(8,128)(2,1)S(1)}, u32[]{:S(2)}, u32[]{:S(2)}) collective-permute-start(bf16[24,2048]{1,0:T(8,128)(2,1)} %get-tuple-element.83), channel_id=1, source_target_pairs={{0,30},{2,32},{4,34},{6,36},{8,38},{10,40},{12,42},{14,44},{16,46}... | collective-permute-start | bytes 294920 | tf_op jit(solution)/shard_map/ppermute | solution.py:117
  584.8 63.8 %collective-permute-start.64 = (bf16[24,2048]{1,0:T(8,128)(2,1)}, bf16[24,2048]{1,0:T(8,128)(2,1)S(1)}, u32[]{:S(2)}, u32[]{:S(2)}) collective-permute-start(bf16[24,2048]{1,0:T(8,128)(2,1)} %get-tuple-element.82), channel_id=1, source_target_pairs={{0,32},{2,34},{4,36},{6,38},{8,40},{10,42},{12,44},{14,46},{16,48}... | collective-permute-start | bytes 294920 | tf_op jit(solution)/shard_map/ppermute | solution.py:117
  (13 other events, 596.1 us)

commit v2 on v1

--- a/solution.py
+++ b/solution.py
@@ -72,6 +72,10 @@
     refs[-1][...] = (sofar_ref[...] + weigh(start, pos_ref, weights_ref, refs[:-1])).astype(BF16)
 
 
+def settle_kernel(in_ref, out_ref):
+    out_ref[...] = jnp.maximum(in_ref[...], 0)
+
+
 def call(kernel, out, operands, limit, specs=None):
     return pl.pallas_call(
         kernel,
@@ -122,15 +126,28 @@
         hidden = (jax.nn.silu(dot(rows, gate_full)) * dot(rows, up_full)).astype(BF16)
         return dot(hidden, down_full).astype(BF16)
 
-    arrived = []
-    for i, d in enumerate(order):
-        arrived.append(shift(send[i * slots : (i + 1) * slots], d))
-    back, result = [], None
-    for lo, hi in ((0, first), (first, len(order))):
+    parts = ((0, first), (first, len(order)))
+
+    def in_turn(lo, hi):
+        out = []
+        while lo < hi:
+            out += [i for i in (hi - 1, hi - 2) if i >= lo]
+            hi -= 2
+            out += [i for i in (lo, lo + 1) if i < hi]
+            lo += 2
+        return out
+
+    arrived, back, result = [None] * len(order), [None] * len(order), None
+    for lo, hi in parts:
+        for i in in_turn(lo, hi):
+            arrived[i] = shift(send[i * slots : (i + 1) * slots], order[i])
+    for lo, hi in parts:
         if result is not None:
             arrived, _ = lax.optimization_barrier((arrived, result))
         result = expert(jnp.concatenate(arrived[lo:hi], axis=0))
-        back += [shift(result[i * slots : (i + 1) * slots], -d) for i, d in enumerate(order[lo:hi])]
+        for i in in_turn(lo, hi):
+            back[i] = shift(result[(i - lo) * slots : (i - lo + 1) * slots], -order[i])
+    pos = call(settle_kernel, sds(pos.shape, I32), (pos,), 1)
     cols = pos.T
     sofar = call(
         first_mix_kernel,

time: 659 us -> 659 us (level)
  no operation moved by 1% of the time
where the time goes in v2:
time: 659 us; the launch traced here: 651 us
  starting transfers between devices  417 us (63%)
  waiting for transfers between devices  191 us (29%)
  matrix products  24.3 us (4%)
  local copies, waits for them, and re-layouts  13.2 us (2%)
    ppermute x62, starting transfers between devices, shift(): lax.ppermute(rows, 'ep', [(i, (i + d) % ep_size) for i in range(ep_size)])  412 us
    ppermute x62, waiting for transfers between devices, shift(): lax.ppermute(rows, 'ep', [(i, (i + d) % ep_size) for i in range(ep_size)])  191 us
    dot_general x4, matrix products, dot(): return jnp.dot(a, b, preferred_element_type=F32)  24.3 us
  transfers between devices with their start and end apart: 65, of which 16 were waited for; matrix products, arithmetic and copies ran while one was open for 2% of the time, Pallas kernels for 0%

profile of v2, /device:TPU:103, one launch (start us, length us, event | category | flops | bytes accessed | tf_op | source)
XLA Modules:
  0.0 650.8 jit_solution(583932561451523875)
XLA Ops:
  4.1 2.0 collective-permute-start
  6.1 4.6 collective-permute-start.2
  10.7 17.1 %collective-permute-start.3 = (bf16[24,2048]{1,0:T(8,128)(2,1)S(1)}, bf16[24,2048]{1,0:T(8,128)(2,1)S(1)}, u32[]{:S(2)}, u32[]{:S(2)}) collective-permute-start(bf16[24,2048]{1,0:T(8,128)(2,1)S(1)} %get-tuple-element.54), channel_id=1, source_target_pairs={{0,60},{2,62},{4,0},{6,2},{8,4},{10,6},{12,8},{14,10},{16,12},{18,... | collective-permute-start | bytes 294920 | tf_op jit(solution)/shard_map/ppermute | solution.py:121
  28.6 4.5 collective-permute-start.5
  33.2 5.4 collective-permute-start.7
  38.8 6.3 collective-permute-start.9
  45.5 2.2 collective-permute-done.6
  47.7 7.9 %collective-permute-start.11 = (bf16[24,2048]{1,0:T(8,128)(2,1)S(1)}, bf16[24,2048]{1,0:T(8,128)(2,1)S(1)}, u32[]{:S(2)}, u32[]{:S(2)}) collective-permute-start(bf16[24,2048]{1,0:T(8,128)(2,1)S(1)} %get-tuple-element.46), channel_id=1, source_target_pairs={{0,52},{2,54},{4,56},{6,58},{8,60},{10,62},{12,0},{14,2},{16,4},{1... | collective-permute-start | bytes 294920 | tf_op jit(solution)/shard_map/ppermute | solution.py:121
  55.5 4.2 collective-permute-start.12
  59.7 5.7 collective-permute-start.13
  65.4 6.2 collective-permute-start.14
  71.6 4.2 collective-permute-start.15
  75.9 5.0 collective-permute-start.16
  80.9 15.3 %collective-permute-done.12 = bf16[24,2048]{1,0:T(8,128)(2,1)S(1)} collective-permute-done((bf16[24,2048]{1,0:T(8,128)(2,1)S(1)}, bf16[24,2048]{1,0:T(8,128)(2,1)S(1)}, u32[]{:S(2)}, u32[]{:S(2)}) %collective-permute-start.12) | collective-permute-done | bytes 98336 | tf_op jit(solution)/shard_map/ppermute | solution.py:121
  97.8 3.2 collective-permute-start.22
  101.2 23.8 %collective-permute-done.16 = bf16[24,2048]{1,0:T(8,128)(2,1)S(1)} collective-permute-done((bf16[24,2048]{1,0:T(8,128)(2,1)S(1)}, bf16[24,2048]{1,0:T(8,128)(2,1)S(1)}, u32[]{:S(2)}, u32[]{:S(2)}) %collective-permute-start.16) | collective-permute-done | bytes 98336 | tf_op jit(solution)/shard_map/ppermute | solution.py:121
  125.0 13.3 %collective-permute-start.19 = (bf16[24,2048]{1,0:T(8,128)(2,1)S(1)}, bf16[24,2048]{1,0:T(8,128)(2,1)S(1)}, u32[]{:S(2)}, u32[]{:S(2)}) collective-permute-start(bf16[24,2048]{1,0:T(8,128)(2,1)S(1)} %get-tuple-element.38), channel_id=1, source_target_pairs={{0,44},{2,46},{4,48},{6,50},{8,52},{10,54},{12,56},{14,58},{16,60}... | collective-permute-start | bytes 294920 | tf_op jit(solution)/shard_map/ppermute | solution.py:121
  138.3 12.5 %collective-permute-done.18 = bf16[24,2048]{1,0:T(8,128)(2,1)S(1)} collective-permute-done((bf16[24,2048]{1,0:T(8,128)(2,1)S(1)}, bf16[24,2048]{1,0:T(8,128)(2,1)S(1)}, u32[]{:S(2)}, u32[]{:S(2)}) %collective-permute-start.18) | collective-permute-done | bytes 98336 | tf_op jit(solution)/shard_map/ppermute | solution.py:121
  152.7 12.4 %collective-permute-start.21 = (bf16[24,2048]{1,0:T(8,128)(2,1)S(1)}, bf16[24,2048]{1,0:T(8,128)(2,1)S(1)}, u32[]{:S(2)}, u32[]{:S(2)}) collective-permute-start(bf16[24,2048]{1,0:T(8,128)(2,1)S(1)} %get-tuple-element.36), channel_id=1, source_target_pairs={{0,42},{2,44},{4,46},{6,48},{8,50},{10,52},{12,54},{14,56},{16,58}... | collective-permute-start | bytes 294920 | tf_op jit(solution)/shard_map/ppermute | solution.py:121
  165.1 16.1 %collective-permute-done.20 = bf16[24,2048]{1,0:T(8,128)(2,1)S(1)} collective-permute-done((bf16[24,2048]{1,0:T(8,128)(2,1)S(1)}, bf16[24,2048]{1,0:T(8,128)(2,1)S(1)}, u32[]{:S(2)}, u32[]{:S(2)}) %collective-permute-start.20) | collective-permute-done | bytes 98336 | tf_op jit(solution)/shard_map/ppermute | solution.py:121
  181.3 14.9 %collective-permute-start.48 = (bf16[24,2048]{1,0:T(8,128)(2,1)S(1)}, bf16[24,2048]{1,0:T(8,128)(2,1)S(1)}, u32[]{:S(2)}, u32[]{:S(2)}) collective-permute-start(bf16[24,2048]{1,0:T(8,128)(2,1)S(1)} %get-tuple-element.34), channel_id=1, source_target_pairs={{0,40},{2,42},{4,44},{6,46},{8,48},{10,50},{12,52},{14,54},{16,56}... | collective-permute-start | bytes 294920 | tf_op jit(solution)/shard_map/ppermute | solution.py:121
  196.3 3.8 collective-permute-done.47
  200.0 18.0 %collective-permute-start.49 = (bf16[24,2048]{1,0:T(8,128)(2,1)S(1)}, bf16[24,2048]{1,0:T(8,128)(2,1)S(1)}, u32[]{:S(2)}, u32[]{:S(2)}) collective-permute-start(bf16[24,2048]{1,0:T(8,128)(2,1)S(1)} %get-tuple-element.33), channel_id=1, source_target_pairs={{0,26},{2,28},{4,30},{6,32},{8,34},{10,36},{12,38},{14,40},{16,42}... | collective-permute-start | bytes 294920 | tf_op jit(solution)/shard_map/ppermute | solution.py:121
  218.5 3.9 fusion.2
  222.4 5.1 collective-permute-done.48
  227.5 13.9 %collective-permute-start.51 = (bf16[24,2048]{1,0:T(8,128)(2,1)}, bf16[24,2048]{1,0:T(8,128)(2,1)S(1)}, u32[]{:S(2)}, u32[]{:S(2)}) collective-permute-start(bf16[24,2048]{1,0:T(8,128)(2,1)} %get-tuple-element.31), channel_id=1, source_target_pairs={{0,28},{2,30},{4,32},{6,34},{8,36},{10,38},{12,40},{14,42},{16,44}... | collective-permute-start | bytes 294920 | tf_op jit(solution)/shard_map/ppermute | solution.py:121
  241.4 4.0 collective-permute-start.52
  245.5 8.6 %collective-permute-start.53 = (bf16[24,2048]{1,0:T(8,128)(2,1)S(1)}, bf16[24,2048]{1,0:T(8,128)(2,1)S(1)}, u32[]{:S(2)}, u32[]{:S(2)}) collective-permute-start(bf16[24,2048]{1,0:T(8,128)(2,1)S(1)} %get-tuple-element.29), channel_id=1, source_target_pairs={{0,30},{2,32},{4,34},{6,36},{8,38},{10,40},{12,42},{14,44},{16,46}... | collective-permute-start | bytes 294920 | tf_op jit(solution)/shard_map/ppermute | solution.py:121
  254.1 10.3 %collective-permute-start.54 = (bf16[24,2048]{1,0:T(8,128)(2,1)S(1)}, bf16[24,2048]{1,0:T(8,128)(2,1)S(1)}, u32[]{:S(2)}, u32[]{:S(2)}) collective-permute-start(bf16[24,2048]{1,0:T(8,128)(2,1)S(1)} %get-tuple-element.28), channel_id=1, source_target_pairs={{0,34},{2,36},{4,38},{6,40},{8,42},{10,44},{12,46},{14,48},{16,50}... | collective-permute-start | bytes 294920 | tf_op jit(solution)/shard_map/ppermute | solution.py:121
  265.8 5.7 collective-permute-start.55
  271.5 9.8 %convolution_convert_fusion = bf16[552,2048]{1,0:T(8,128)(2,1)S(1)} fusion(bf16[512,2048]{1,0:T(8,128)(2,1)} %copy-done.11, bf16[512,2048]{1,0:T(8,128)(2,1)} %bitcast.18, f32[552,1024]{1,0:T(8,128)} %fusion.2, bf16[552,2048]{1,0:T(8,128)(2,1)} %copy-done.4, bf16[2048,512]{1,0:T(8,128)(2,1)} %copy-done.10, bf16[2048,512]{1,0:T(8,128)(2,1)} %bitcast.21), kind=kOutput, calls=%fused_computation.3 | convolution fusion | flops 4651810816 | bytes 15171584 | tf_op jit(solution)/shard_map/dot_general | solution.py:16
  281.3 24.2 %collective-permute-done.51 = bf16[24,2048]{1,0:T(8,128)(2,1)S(1)} collective-permute-done((bf16[24,2048]{1,0:T(8,128)(2,1)}, bf16[24,2048]{1,0:T(8,128)(2,1)S(1)}, u32[]{:S(2)}, u32[]{:S(2)}) %collective-permute-start.51) | collective-permute-done | bytes 98336 | tf_op jit(solution)/shard_map/ppermute | solution.py:121
  305.6 17.6 %collective-permute-done.54 = bf16[24,2048]{1,0:T(8,128)(2,1)S(1)} collective-permute-done((bf16[24,2048]{1,0:T(8,128)(2,1)S(1)}, bf16[24,2048]{1,0:T(8,128)(2,1)S(1)}, u32[]{:S(2)}, u32[]{:S(2)}) %collective-permute-start.54) | collective-permute-done | bytes 98336 | tf_op jit(solution)/shard_map/ppermute | solution.py:121
  329.0 4.5 fusion.1
  333.5 6.0 fusion.5
  340.3 4.4 collective-permute-start.56
  344.7 13.6 %collective-permute-start.57 = (bf16[24,2048]{1,0:T(8,128)(2,1)S(1)}, bf16[24,2048]{1,0:T(8,128)(2,1)S(1)}, u32[]{:S(2)}, u32[]{:S(2)}) collective-permute-start(bf16[24,2048]{1,0:T(8,128)(2,1)S(1)} %get-tuple-element.89), channel_id=1, source_target_pairs={{0,24},{2,26},{4,28},{6,30},{8,32},{10,34},{12,36},{14,38},{16,40}... | collective-permute-start | bytes 294920 | tf_op jit(solution)/shard_map/ppermute | solution.py:121
  358.3 5.2 collective-permute-start.58
  363.5 10.7 %collective-permute-start.59 = (bf16[24,2048]{1,0:T(8,128)(2,1)S(1)}, bf16[24,2048]{1,0:T(8,128)(2,1)S(1)}, u32[]{:S(2)}, u32[]{:S(2)}) collective-permute-start(bf16[24,2048]{1,0:T(8,128)(2,1)S(1)} %get-tuple-element.87), channel_id=1, source_target_pairs={{0,26},{2,28},{4,30},{6,32},{8,34},{10,36},{12,38},{14,40},{16,42}... | collective-permute-start | bytes 294920 | tf_op jit(solution)/shard_map/ppermute | solution.py:121
  374.3 12.1 %collective-permute-start.28 = (bf16[24,2048]{1,0:T(8,128)(2,1)S(1)}, bf16[24,2048]{1,0:T(8,128)(2,1)S(1)}, u32[]{:S(2)}, u32[]{:S(2)}) collective-permute-start(bf16[24,2048]{1,0:T(8,128)(2,1)S(1)} %get-tuple-element.77), channel_id=1, source_target_pairs={{0,4},{2,6},{4,8},{6,10},{8,12},{10,14},{12,16},{14,18},{16,20},{1... | collective-permute-start | bytes 294920 | tf_op jit(solution)/shard_map/ppermute | solution.py:121
  386.4 4.5 collective-permute-start.30
  390.9 22.9 %collective-permute-start.31 = (bf16[24,2048]{1,0:T(8,128)(2,1)S(1)}, bf16[24,2048]{1,0:T(8,128)(2,1)S(1)}, u32[]{:S(2)}, u32[]{:S(2)}) collective-permute-start(bf16[24,2048]{1,0:T(8,128)(2,1)S(1)} %get-tuple-element.74), channel_id=1, source_target_pairs={{0,56},{2,58},{4,60},{6,62},{8,0},{10,2},{12,4},{14,6},{16,8},{18,... | collective-permute-start | bytes 294920 | tf_op jit(solution)/shard_map/ppermute | solution.py:121
  413.9 2.2 collective-permute-start.32
  416.1 10.0 %collective-permute-start.33 = (bf16[24,2048]{1,0:T(8,128)(2,1)S(1)}, bf16[24,2048]{1,0:T(8,128)(2,1)S(1)}, u32[]{:S(2)}, u32[]{:S(2)}) collective-permute-start(bf16[24,2048]{1,0:T(8,128)(2,1)S(1)} %get-tuple-element.72), channel_id=1, source_target_pairs={{0,54},{2,56},{4,58},{6,60},{8,62},{10,0},{12,2},{14,4},{16,6},{18... | collective-permute-start | bytes 294920 | tf_op jit(solution)/shard_map/ppermute | solution.py:121
  426.2 9.3 %collective-permute-start.35 = (bf16[24,2048]{1,0:T(8,128)(2,1)S(1)}, bf16[24,2048]{1,0:T(8,128)(2,1)S(1)}, u32[]{:S(2)}, u32[]{:S(2)}) collective-permute-start(bf16[24,2048]{1,0:T(8,128)(2,1)S(1)} %get-tuple-element.70), channel_id=1, source_target_pairs={{0,52},{2,54},{4,56},{6,58},{8,60},{10,62},{12,0},{14,2},{16,4},{1... | collective-permute-start | bytes 294920 | tf_op jit(solution)/shard_map/ppermute | solution.py:121
  435.5 2.4 collective-permute-start.36
  438.0 4.7 collective-permute-start.37
  442.7 4.6 collective-permute-start.38
  447.3 7.0 %collective-permute-start.39 = (bf16[24,2048]{1,0:T(8,128)(2,1)S(1)}, bf16[24,2048]{1,0:T(8,128)(2,1)S(1)}, u32[]{:S(2)}, u32[]{:S(2)}) collective-permute-start(bf16[24,2048]{1,0:T(8,128)(2,1)S(1)} %get-tuple-element.66), channel_id=1, source_target_pairs={{0,48},{2,50},{4,52},{6,54},{8,56},{10,58},{12,60},{14,62},{16,0},... | collective-permute-start | bytes 294920 | tf_op jit(solution)/shard_map/ppermute | solution.py:121
  454.3 3.4 collective-permute-start.40
  457.7 13.3 %collective-permute-start.41 = (bf16[24,2048]{1,0:T(8,128)(2,1)S(1)}, bf16[24,2048]{1,0:T(8,128)(2,1)S(1)}, u32[]{:S(2)}, u32[]{:S(2)}) collective-permute-start(bf16[24,2048]{1,0:T(8,128)(2,1)S(1)} %get-tuple-element.64), channel_id=1, source_target_pairs={{0,46},{2,48},{4,50},{6,52},{8,54},{10,56},{12,58},{14,60},{16,62}... | collective-permute-start | bytes 294920 | tf_op jit(solution)/shard_map/ppermute | solution.py:121
  471.9 13.8 %collective-permute-start.43 = (bf16[24,2048]{1,0:T(8,128)(2,1)S(1)}, bf16[24,2048]{1,0:T(8,128)(2,1)S(1)}, u32[]{:S(2)}, u32[]{:S(2)}) collective-permute-start(bf16[24,2048]{1,0:T(8,128)(2,1)S(1)} %get-tuple-element.62), channel_id=1, source_target_pairs={{0,44},{2,46},{4,48},{6,50},{8,52},{10,54},{12,56},{14,58},{16,60}... | collective-permute-start | bytes 294920 | tf_op jit(solution)/shard_map/ppermute | solution.py:121
  485.7 12.8 %collective-permute-done.39.refs_15_ = bf16[24,2048]{1,0:T(8,128)(2,1)S(1)} collective-permute-done((bf16[24,2048]{1,0:T(8,128)(2,1)S(1)}, bf16[24,2048]{1,0:T(8,128)(2,1)S(1)}, u32[]{:S(2)}, u32[]{:S(2)}) %collective-permute-start.39) | collective-permute-done | bytes 98336 | tf_op jit(solution)/shard_map/ppermute | solution.py:121
  499.6 19.2 %collective-permute-start.45 = (bf16[24,2048]{1,0:T(8,128)(2,1)S(1)}, bf16[24,2048]{1,0:T(8,128)(2,1)S(1)}, u32[]{:S(2)}, u32[]{:S(2)}) collective-permute-start(bf16[24,2048]{1,0:T(8,128)(2,1)S(1)} %get-tuple-element.60), channel_id=1, source_target_pairs={{0,42},{2,44},{4,46},{6,48},{8,50},{10,52},{12,54},{14,56},{16,58}... | collective-permute-start | bytes 294920 | tf_op jit(solution)/shard_map/ppermute | solution.py:121
  518.9 8.2 %collective-permute-done.43.refs_19_ = bf16[24,2048]{1,0:T(8,128)(2,1)S(1)} collective-permute-done((bf16[24,2048]{1,0:T(8,128)(2,1)S(1)}, bf16[24,2048]{1,0:T(8,128)(2,1)S(1)}, u32[]{:S(2)}, u32[]{:S(2)}) %collective-permute-start.43) | collective-permute-done | bytes 98336 | tf_op jit(solution)/shard_map/ppermute | solution.py:121
  527.1 10.0 %collective-permute-start.27 = (bf16[24,2048]{1,0:T(8,128)(2,1)S(1)}, bf16[24,2048]{1,0:T(8,128)(2,1)S(1)}, u32[]{:S(2)}, u32[]{:S(2)}) collective-permute-start(bf16[24,2048]{1,0:T(8,128)(2,1)S(1)} %get-tuple-element.78), channel_id=1, source_target_pairs={{0,60},{2,62},{4,0},{6,2},{8,4},{10,6},{12,8},{14,10},{16,12},{18,... | collective-permute-start | bytes 294920 | tf_op jit(solution)/shard_map/ppermute | solution.py:121
  537.1 27.2 %collective-permute-start.60 = (bf16[24,2048]{1,0:T(8,128)(2,1)}, bf16[24,2048]{1,0:T(8,128)(2,1)S(1)}, u32[]{:S(2)}, u32[]{:S(2)}) collective-permute-start(bf16[24,2048]{1,0:T(8,128)(2,1)} %get-tuple-element.86), channel_id=1, source_target_pairs={{0,36},{2,38},{4,40},{6,42},{8,44},{10,46},{12,48},{14,50},{16,52}... | collective-permute-start | bytes 294920 | tf_op jit(solution)/shard_map/ppermute | solution.py:121
  564.3 19.2 %collective-permute-start.62 = (bf16[24,2048]{1,0:T(8,128)(2,1)}, bf16[24,2048]{1,0:T(8,128)(2,1)S(1)}, u32[]{:S(2)}, u32[]{:S(2)}) collective-permute-start(bf16[24,2048]{1,0:T(8,128)(2,1)} %get-tuple-element.84), channel_id=1, source_target_pairs={{0,34},{2,36},{4,38},{6,40},{8,42},{10,44},{12,46},{14,48},{16,50}... | collective-permute-start | bytes 294920 | tf_op jit(solution)/shard_map/ppermute | solution.py:121
  584.8 15.1 %collective-permute-start.64 = (bf16[24,2048]{1,0:T(8,128)(2,1)}, bf16[24,2048]{1,0:T(8,128)(2,1)S(1)}, u32[]{:S(2)}, u32[]{:S(2)}) collective-permute-start(bf16[24,2048]{1,0:T(8,128)(2,1)} %get-tuple-element.82), channel_id=1, source_target_pairs={{0,32},{2,34},{4,36},{6,38},{8,40},{10,42},{12,44},{14,46},{16,48}... | collective-permute-start | bytes 294920 | tf_op jit(solution)/shard_map/ppermute | solution.py:121
  600.1 1.9 shard_map.75.refs_2_
  602.0 15.9 %collective-permute-done.62.refs_9_ = bf16[24,2048]{1,0:T(8,128)(2,1)S(1)} collective-permute-done((bf16[24,2048]{1,0:T(8,128)(2,1)}, bf16[24,2048]{1,0:T(8,128)(2,1)S(1)}, u32[]{:S(2)}, u32[]{:S(2)}) %collective-permute-start.62) | collective-permute-done | bytes 98336 | tf_op jit(solution)/shard_map/ppermute | solution.py:121
  618.0 5.7 collective-permute-done.63.refs_10_
  623.7 24.8 %collective-permute-done.64.refs_11_ = bf16[24,2048]{1,0:T(8,128)(2,1)S(1)} collective-permute-done((bf16[24,2048]{1,0:T(8,128)(2,1)}, bf16[24,2048]{1,0:T(8,128)(2,1)S(1)}, u32[]{:S(2)}, u32[]{:S(2)}) %collective-permute-start.64) | collective-permute-done | bytes 98336 | tf_op jit(solution)/shard_map/ppermute | solution.py:121
  648.5 1.9 shard_map.76
  (136 shorter events, 21.7 us)
Async XLA Ops:
  4.1 24.5 %collective-permute-start = (bf16[24,2048]{1,0:T(8,128)(2,1)S(1)}, bf16[24,2048]{1,0:T(8,128)(2,1)S(1)}, u32[]{:S(2)}, u32[]{:S(2)}) collective-permute-start(bf16[24,2048]{1,0:T(8,128)(2,1)S(1)} %get-tuple-element.57), channel_id=1, source_target_pairs={{0,2},{2,4},{4,6},{6,8},{8,10},{10,12},{12,14},{14,16},{16,18},{18... | collective-permute-start | bytes 294920 | tf_op jit(solution)/shard_map/ppermute | solution.py:121
  6.1 27.0 %collective-permute-start.1 = (bf16[24,2048]{1,0:T(8,128)(2,1)S(1)}, bf16[24,2048]{1,0:T(8,128)(2,1)S(1)}, u32[]{:S(2)}, u32[]{:S(2)}) collective-permute-start(bf16[24,2048]{1,0:T(8,128)(2,1)S(1)} %get-tuple-element.56), channel_id=1, source_target_pairs={{0,62},{2,0},{4,2},{6,4},{8,6},{10,8},{12,10},{14,12},{16,14},{18,... | collective-permute-start | bytes 294920 | tf_op jit(solution)/shard_map/ppermute | solution.py:121
  6.1 27.2 %collective-permute-start.2 = (bf16[24,2048]{1,0:T(8,128)(2,1)S(1)}, bf16[24,2048]{1,0:T(8,128)(2,1)S(1)}, u32[]{:S(2)}, u32[]{:S(2)}) collective-permute-start(bf16[24,2048]{1,0:T(8,128)(2,1)S(1)} %get-tuple-element.55), channel_id=1, source_target_pairs={{0,4},{2,6},{4,8},{6,10},{8,12},{10,14},{12,16},{14,18},{16,20},{1... | collective-permute-start | bytes 294920 | tf_op jit(solution)/shard_map/ppermute | solution.py:121
  10.7 28.0 %collective-permute-start.3 = (bf16[24,2048]{1,0:T(8,128)(2,1)S(1)}, bf16[24,2048]{1,0:T(8,128)(2,1)S(1)}, u32[]{:S(2)}, u32[]{:S(2)}) collective-permute-start(bf16[24,2048]{1,0:T(8,128)(2,1)S(1)} %get-tuple-element.54), channel_id=1, source_target_pairs={{0,60},{2,62},{4,0},{6,2},{8,4},{10,6},{12,8},{14,10},{16,12},{18,... | collective-permute-start | bytes 294920 | tf_op jit(solution)/shard_map/ppermute | solution.py:121
  28.6 16.6 %collective-permute-start.5 = (bf16[24,2048]{1,0:T(8,128)(2,1)S(1)}, bf16[24,2048]{1,0:T(8,128)(2,1)S(1)}, u32[]{:S(2)}, u32[]{:S(2)}) collective-permute-start(bf16[24,2048]{1,0:T(8,128)(2,1)S(1)} %get-tuple-element.52), channel_id=1, source_target_pairs={{0,58},{2,60},{4,62},{6,0},{8,2},{10,4},{12,6},{14,8},{16,10},{18,... | collective-permute-start | bytes 294920 | tf_op jit(solution)/shard_map/ppermute | solution.py:121
  33.1 14.6 %collective-permute-start.6 = (bf16[24,2048]{1,0:T(8,128)(2,1)S(1)}, bf16[24,2048]{1,0:T(8,128)(2,1)S(1)}, u32[]{:S(2)}, u32[]{:S(2)}) collective-permute-start(bf16[24,2048]{1,0:T(8,128)(2,1)S(1)} %get-tuple-element.51), channel_id=1, source_target_pairs={{0,8},{2,10},{4,12},{6,14},{8,16},{10,18},{12,20},{14,22},{16,24},... | collective-permute-start | bytes 294920 | tf_op jit(solution)/shard_map/ppermute | solution.py:121
  33.2 22.3 %collective-permute-start.7 = (bf16[24,2048]{1,0:T(8,128)(2,1)S(1)}, bf16[24,2048]{1,0:T(8,128)(2,1)S(1)}, u32[]{:S(2)}, u32[]{:S(2)}) collective-permute-start(bf16[24,2048]{1,0:T(8,128)(2,1)S(1)} %get-tuple-element.50), channel_id=1, source_target_pairs={{0,56},{2,58},{4,60},{6,62},{8,0},{10,2},{12,4},{14,6},{16,8},{18,... | collective-permute-start | bytes 294920 | tf_op jit(solution)/shard_map/ppermute | solution.py:121
  38.7 21.1 %collective-permute-start.8 = (bf16[24,2048]{1,0:T(8,128)(2,1)S(1)}, bf16[24,2048]{1,0:T(8,128)(2,1)S(1)}, u32[]{:S(2)}, u32[]{:S(2)}) collective-permute-start(bf16[24,2048]{1,0:T(8,128)(2,1)S(1)} %get-tuple-element.49), channel_id=1, source_target_pairs={{0,10},{2,12},{4,14},{6,16},{8,18},{10,20},{12,22},{14,24},{16,26}... | collective-permute-start | bytes 294920 | tf_op jit(solution)/shard_map/ppermute | solution.py:121
  38.8 26.6 %collective-permute-start.9 = (bf16[24,2048]{1,0:T(8,128)(2,1)S(1)}, bf16[24,2048]{1,0:T(8,128)(2,1)S(1)}, u32[]{:S(2)}, u32[]{:S(2)}) collective-permute-start(bf16[24,2048]{1,0:T(8,128)(2,1)S(1)} %get-tuple-element.48), channel_id=1, source_target_pairs={{0,54},{2,56},{4,58},{6,60},{8,62},{10,0},{12,2},{14,4},{16,6},{18... | collective-permute-start | bytes 294920 | tf_op jit(solution)/shard_map/ppermute | solution.py:121
  45.2 26.4 %collective-permute-start.10 = (bf16[24,2048]{1,0:T(8,128)(2,1)S(1)}, bf16[24,2048]{1,0:T(8,128)(2,1)S(1)}, u32[]{:S(2)}, u32[]{:S(2)}) collective-permute-start(bf16[24,2048]{1,0:T(8,128)(2,1)S(1)} %get-tuple-element.47), channel_id=1, source_target_pairs={{0,12},{2,14},{4,16},{6,18},{8,20},{10,22},{12,24},{14,26},{16,28}... | collective-permute-start | bytes 294920 | tf_op jit(solution)/shard_map/ppermute | solution.py:121
  47.7 28.2 %collective-permute-start.11 = (bf16[24,2048]{1,0:T(8,128)(2,1)S(1)}, bf16[24,2048]{1,0:T(8,128)(2,1)S(1)}, u32[]{:S(2)}, u32[]{:S(2)}) collective-permute-start(bf16[24,2048]{1,0:T(8,128)(2,1)S(1)} %get-tuple-element.46), channel_id=1, source_target_pairs={{0,52},{2,54},{4,56},{6,58},{8,60},{10,62},{12,0},{14,2},{16,4},{1... | collective-permute-start | bytes 294920 | tf_op jit(solution)/shard_map/ppermute | solution.py:121
  55.5 40.7 %collective-permute-start.12 = (bf16[24,2048]{1,0:T(8,128)(2,1)S(1)}, bf16[24,2048]{1,0:T(8,128)(2,1)S(1)}, u32[]{:S(2)}, u32[]{:S(2)}) collective-permute-start(bf16[24,2048]{1,0:T(8,128)(2,1)S(1)} %get-tuple-element.45), channel_id=1, source_target_pairs={{0,14},{2,16},{4,18},{6,20},{8,22},{10,24},{12,26},{14,28},{16,30}... | collective-permute-start | bytes 294920 | tf_op jit(solution)/shard_map/ppermute | solution.py:121
  59.7 37.8 %collective-permute-start.13 = (bf16[24,2048]{1,0:T(8,128)(2,1)S(1)}, bf16[24,2048]{1,0:T(8,128)(2,1)S(1)}, u32[]{:S(2)}, u32[]{:S(2)}) collective-permute-start(bf16[24,2048]{1,0:T(8,128)(2,1)S(1)} %get-tuple-element.44), channel_id=1, source_target_pairs={{0,50},{2,52},{4,54},{6,56},{8,58},{10,60},{12,62},{14,0},{16,2},{... | collective-permute-start | bytes 294920 | tf_op jit(solution)/shard_map/ppermute | solution.py:121
  65.4 32.3 %collective-permute-start.14 = (bf16[24,2048]{1,0:T(8,128)(2,1)S(1)}, bf16[24,2048]{1,0:T(8,128)(2,1)S(1)}, u32[]{:S(2)}, u32[]{:S(2)}) collective-permute-start(bf16[24,2048]{1,0:T(8,128)(2,1)S(1)} %get-tuple-element.43), channel_id=1, source_target_pairs={{0,16},{2,18},{4,20},{6,22},{8,24},{10,26},{12,28},{14,30},{16,32}... | collective-permute-start | bytes 294920 | tf_op jit(solution)/shard_map/ppermute | solution.py:121
  71.6 29.3 %collective-permute-start.15 = (bf16[24,2048]{1,0:T(8,128)(2,1)S(1)}, bf16[24,2048]{1,0:T(8,128)(2,1)S(1)}, u32[]{:S(2)}, u32[]{:S(2)}) collective-permute-start(bf16[24,2048]{1,0:T(8,128)(2,1)S(1)} %get-tuple-element.42), channel_id=1, source_target_pairs={{0,48},{2,50},{4,52},{6,54},{8,56},{10,58},{12,60},{14,62},{16,0},... | collective-permute-start | bytes 294920 | tf_op jit(solution)/shard_map/ppermute | solution.py:121
  75.9 49.1 %collective-permute-start.16 = (bf16[24,2048]{1,0:T(8,128)(2,1)S(1)}, bf16[24,2048]{1,0:T(8,128)(2,1)S(1)}, u32[]{:S(2)}, u32[]{:S(2)}) collective-permute-start(bf16[24,2048]{1,0:T(8,128)(2,1)S(1)} %get-tuple-element.41), channel_id=1, source_target_pairs={{0,18},{2,20},{4,22},{6,24},{8,26},{10,28},{12,30},{14,32},{16,34}... | collective-permute-start | bytes 294920 | tf_op jit(solution)/shard_map/ppermute | solution.py:121
  96.2 121.8 %collective-permute-start.23 = (bf16[2048,512]{1,0:T(8,128)(2,1)S(1)}, bf16[2048,512]{1,0:T(8,128)(2,1)S(1)}, u32[]{:S(2)}, u32[]{:S(2)}) collective-permute-start(bf16[2048,512]{1,0:T(8,128)(2,1)S(1)} %bitcast.16), channel_id=1, source_target_pairs={{0,1},{1,0},{2,3},{3,2},{4,5},{5,4},{6,7},{7,6},{8,9},{9,8},{10,11... | collective-permute-start | bytes 6291464 | tf_op jit(solution)/shard_map/ppermute | solution.py:116
  97.6 27.4 %collective-permute-start.17 = (bf16[24,2048]{1,0:T(8,128)(2,1)S(1)}, bf16[24,2048]{1,0:T(8,128)(2,1)S(1)}, u32[]{:S(2)}, u32[]{:S(2)}) collective-permute-start(bf16[24,2048]{1,0:T(8,128)(2,1)S(1)} %get-tuple-element.40), channel_id=1, source_target_pairs={{0,46},{2,48},{4,50},{6,52},{8,54},{10,56},{12,58},{14,60},{16,62}... | collective-permute-start | bytes 294920 | tf_op jit(solution)/shard_map/ppermute | solution.py:121
  97.8 156.4 %collective-permute-start.22 = (bf16[2048,512]{1,0:T(8,128)(2,1)S(1)}, bf16[2048,512]{1,0:T(8,128)(2,1)S(1)}, u32[]{:S(2)}, u32[]{:S(2)}) collective-permute-start(bf16[2048,512]{1,0:T(8,128)(2,1)S(1)} %bitcast.23), channel_id=1, source_target_pairs={{0,1},{1,0},{2,3},{3,2},{4,5},{5,4},{6,7},{7,6},{8,9},{9,8},{10,11... | collective-permute-start | bytes 6291464 | tf_op jit(solution)/shard_map/ppermute | solution.py:116
  101.0 163.4 %collective-permute-start.24 = (bf16[512,2048]{1,0:T(8,128)(2,1)S(1)}, bf16[512,2048]{1,0:T(8,128)(2,1)S(1)}, u32[]{:S(2)}, u32[]{:S(2)}) collective-permute-start(bf16[512,2048]{1,0:T(8,128)(2,1)S(1)} %bitcast.20), channel_id=1, source_target_pairs={{0,1},{1,0},{2,3},{3,2},{4,5},{5,4},{6,7},{7,6},{8,9},{9,8},{10,11... | collective-permute-start | bytes 6291464 | tf_op jit(solution)/shard_map/ppermute | solution.py:116
  125.0 25.9 %collective-permute-start.18 = (bf16[24,2048]{1,0:T(8,128)(2,1)S(1)}, bf16[24,2048]{1,0:T(8,128)(2,1)S(1)}, u32[]{:S(2)}, u32[]{:S(2)}) collective-permute-start(bf16[24,2048]{1,0:T(8,128)(2,1)S(1)} %get-tuple-element.39), channel_id=1, source_target_pairs={{0,20},{2,22},{4,24},{6,26},{8,28},{10,30},{12,32},{14,34},{16,36}... | collective-permute-start | bytes 294920 | tf_op jit(solution)/shard_map/ppermute | solution.py:121
  125.0 27.7 %collective-permute-start.19 = (bf16[24,2048]{1,0:T(8,128)(2,1)S(1)}, bf16[24,2048]{1,0:T(8,128)(2,1)S(1)}, u32[]{:S(2)}, u32[]{:S(2)}) collective-permute-start(bf16[24,2048]{1,0:T(8,128)(2,1)S(1)} %get-tuple-element.38), channel_id=1, source_target_pairs={{0,44},{2,46},{4,48},{6,50},{8,52},{10,54},{12,56},{14,58},{16,60}... | collective-permute-start | bytes 294920 | tf_op jit(solution)/shard_map/ppermute | solution.py:121
  150.8 30.3 %collective-permute-start.20 = (bf16[24,2048]{1,0:T(8,128)(2,1)S(1)}, bf16[24,2048]{1,0:T(8,128)(2,1)S(1)}, u32[]{:S(2)}, u32[]{:S(2)}) collective-permute-start(bf16[24,2048]{1,0:T(8,128)(2,1)S(1)} %get-tuple-element.37), channel_id=1, source_target_pairs={{0,22},{2,24},{4,26},{6,28},{8,30},{10,32},{12,34},{14,36},{16,38}... | collective-permute-start | bytes 294920 | tf_op jit(solution)/shard_map/ppermute | solution.py:121
  152.7 28.6 %collective-permute-start.21 = (bf16[24,2048]{1,0:T(8,128)(2,1)S(1)}, bf16[24,2048]{1,0:T(8,128)(2,1)S(1)}, u32[]{:S(2)}, u32[]{:S(2)}) collective-permute-start(bf16[24,2048]{1,0:T(8,128)(2,1)S(1)} %get-tuple-element.36), channel_id=1, source_target_pairs={{0,42},{2,44},{4,46},{6,48},{8,50},{10,52},{12,54},{14,56},{16,58}... | collective-permute-start | bytes 294920 | tf_op jit(solution)/shard_map/ppermute | solution.py:121
  181.1 18.9 %collective-permute-start.47 = (bf16[24,2048]{1,0:T(8,128)(2,1)S(1)}, bf16[24,2048]{1,0:T(8,128)(2,1)S(1)}, u32[]{:S(2)}, u32[]{:S(2)}) collective-permute-start(bf16[24,2048]{1,0:T(8,128)(2,1)S(1)} %get-tuple-element.35), channel_id=1, source_target_pairs={{0,24},{2,26},{4,28},{6,30},{8,32},{10,34},{12,36},{14,38},{16,40}... | collective-permute-start | bytes 294920 | tf_op jit(solution)/shard_map/ppermute | solution.py:121
  181.3 46.2 %collective-permute-start.48 = (bf16[24,2048]{1,0:T(8,128)(2,1)S(1)}, bf16[24,2048]{1,0:T(8,128)(2,1)S(1)}, u32[]{:S(2)}, u32[]{:S(2)}) collective-permute-start(bf16[24,2048]{1,0:T(8,128)(2,1)S(1)} %get-tuple-element.34), channel_id=1, source_target_pairs={{0,40},{2,42},{4,44},{6,46},{8,48},{10,50},{12,52},{14,54},{16,56}... | collective-permute-start | bytes 294920 | tf_op jit(solution)/shard_map/ppermute | solution.py:121
  200.0 41.4 %collective-permute-start.49 = (bf16[24,2048]{1,0:T(8,128)(2,1)S(1)}, bf16[24,2048]{1,0:T(8,128)(2,1)S(1)}, u32[]{:S(2)}, u32[]{:S(2)}) collective-permute-start(bf16[24,2048]{1,0:T(8,128)(2,1)S(1)} %get-tuple-element.33), channel_id=1, source_target_pairs={{0,26},{2,28},{4,30},{6,32},{8,34},{10,36},{12,38},{14,40},{16,42}... | collective-permute-start | bytes 294920 | tf_op jit(solution)/shard_map/ppermute | solution.py:121
  218.1 27.4 %collective-permute-start.50 = (bf16[24,2048]{1,0:T(8,128)(2,1)S(1)}, bf16[24,2048]{1,0:T(8,128)(2,1)S(1)}, u32[]{:S(2)}, u32[]{:S(2)}) collective-permute-start(bf16[24,2048]{1,0:T(8,128)(2,1)S(1)} %get-tuple-element.32), channel_id=1, source_target_pairs={{0,38},{2,40},{4,42},{6,44},{8,46},{10,48},{12,50},{14,52},{16,54}... | collective-permute-start | bytes 294920 | tf_op jit(solution)/shard_map/ppermute | solution.py:121
  227.5 78.1 %collective-permute-start.51 = (bf16[24,2048]{1,0:T(8,128)(2,1)}, bf16[24,2048]{1,0:T(8,128)(2,1)S(1)}, u32[]{:S(2)}, u32[]{:S(2)}) collective-permute-start(bf16[24,2048]{1,0:T(8,128)(2,1)} %get-tuple-element.31), channel_id=1, source_target_pairs={{0,28},{2,30},{4,32},{6,34},{8,36},{10,38},{12,40},{14,42},{16,44}... | collective-permute-start | bytes 294920 | tf_op jit(solution)/shard_map/ppermute | solution.py:121
  241.4 64.1 %collective-permute-start.52 = (bf16[24,2048]{1,0:T(8,128)(2,1)S(1)}, bf16[24,2048]{1,0:T(8,128)(2,1)S(1)}, u32[]{:S(2)}, u32[]{:S(2)}) collective-permute-start(bf16[24,2048]{1,0:T(8,128)(2,1)S(1)} %get-tuple-element.30), channel_id=1, source_target_pairs={{0,36},{2,38},{4,40},{6,42},{8,44},{10,46},{12,48},{14,50},{16,52}... | collective-permute-start | bytes 294920 | tf_op jit(solution)/shard_map/ppermute | solution.py:121
  245.5 60.1 %collective-permute-start.53 = (bf16[24,2048]{1,0:T(8,128)(2,1)S(1)}, bf16[24,2048]{1,0:T(8,128)(2,1)S(1)}, u32[]{:S(2)}, u32[]{:S(2)}) collective-permute-start(bf16[24,2048]{1,0:T(8,128)(2,1)S(1)} %get-tuple-element.29), channel_id=1, source_target_pairs={{0,30},{2,32},{4,34},{6,36},{8,38},{10,40},{12,42},{14,44},{16,46}... | collective-permute-start | bytes 294920 | tf_op jit(solution)/shard_map/ppermute | solution.py:121
  254.1 69.0 %collective-permute-start.54 = (bf16[24,2048]{1,0:T(8,128)(2,1)S(1)}, bf16[24,2048]{1,0:T(8,128)(2,1)S(1)}, u32[]{:S(2)}, u32[]{:S(2)}) collective-permute-start(bf16[24,2048]{1,0:T(8,128)(2,1)S(1)} %get-tuple-element.28), channel_id=1, source_target_pairs={{0,34},{2,36},{4,38},{6,40},{8,42},{10,44},{12,46},{14,48},{16,50}... | collective-permute-start | bytes 294920 | tf_op jit(solution)/shard_map/ppermute | solution.py:121
  265.8 57.4 %collective-permute-start.55 = (bf16[24,2048]{1,0:T(8,128)(2,1)S(1)}, bf16[24,2048]{1,0:T(8,128)(2,1)S(1)}, u32[]{:S(2)}, u32[]{:S(2)}) collective-permute-start(bf16[24,2048]{1,0:T(8,128)(2,1)S(1)} %get-tuple-element.27), channel_id=1, source_target_pairs={{0,32},{2,34},{4,36},{6,38},{8,40},{10,42},{12,44},{14,46},{16,48}... | collective-permute-start | bytes 294920 | tf_op jit(solution)/shard_map/ppermute | solution.py:121
  340.3 46.1 %collective-permute-start.56 = (bf16[24,2048]{1,0:T(8,128)(2,1)S(1)}, bf16[24,2048]{1,0:T(8,128)(2,1)S(1)}, u32[]{:S(2)}, u32[]{:S(2)}) collective-permute-start(bf16[24,2048]{1,0:T(8,128)(2,1)S(1)} %get-tuple-element.90), channel_id=1, source_target_pairs={{0,40},{2,42},{4,44},{6,46},{8,48},{10,50},{12,52},{14,54},{16,56}... | collective-permute-start | bytes 294920 | tf_op jit(solution)/shard_map/ppermute | solution.py:121
  344.7 41.7 %collective-permute-start.57 = (bf16[24,2048]{1,0:T(8,128)(2,1)S(1)}, bf16[24,2048]{1,0:T(8,128)(2,1)S(1)}, u32[]{:S(2)}, u32[]{:S(2)}) collective-permute-start(bf16[24,2048]{1,0:T(8,128)(2,1)S(1)} %get-tuple-element.89), channel_id=1, source_target_pairs={{0,24},{2,26},{4,28},{6,30},{8,32},{10,34},{12,36},{14,38},{16,40}... | collective-permute-start | bytes 294920 | tf_op jit(solution)/shard_map/ppermute | solution.py:121
  358.3 32.6 %collective-permute-start.58 = (bf16[24,2048]{1,0:T(8,128)(2,1)S(1)}, bf16[24,2048]{1,0:T(8,128)(2,1)S(1)}, u32[]{:S(2)}, u32[]{:S(2)}) collective-permute-start(bf16[24,2048]{1,0:T(8,128)(2,1)S(1)} %get-tuple-element.88), channel_id=1, source_target_pairs={{0,38},{2,40},{4,42},{6,44},{8,46},{10,48},{12,50},{14,52},{16,54}... | collective-permute-start | bytes 294920 | tf_op jit(solution)/shard_map/ppermute | solution.py:121
  363.5 50.4 %collective-permute-start.59 = (bf16[24,2048]{1,0:T(8,128)(2,1)S(1)}, bf16[24,2048]{1,0:T(8,128)(2,1)S(1)}, u32[]{:S(2)}, u32[]{:S(2)}) collective-permute-start(bf16[24,2048]{1,0:T(8,128)(2,1)S(1)} %get-tuple-element.87), channel_id=1, source_target_pairs={{0,26},{2,28},{4,30},{6,32},{8,34},{10,36},{12,38},{14,40},{16,42}... | collective-permute-start | bytes 294920 | tf_op jit(solution)/shard_map/ppermute | solution.py:121
  374.3 41.8 %collective-permute-start.28 = (bf16[24,2048]{1,0:T(8,128)(2,1)S(1)}, bf16[24,2048]{1,0:T(8,128)(2,1)S(1)}, u32[]{:S(2)}, u32[]{:S(2)}) collective-permute-start(bf16[24,2048]{1,0:T(8,128)(2,1)S(1)} %get-tuple-element.77), channel_id=1, source_target_pairs={{0,4},{2,6},{4,8},{6,10},{8,12},{10,14},{12,16},{14,18},{16,20},{1... | collective-permute-start | bytes 294920 | tf_op jit(solution)/shard_map/ppermute | solution.py:121
  386.4 39.7 %collective-permute-start.29 = (bf16[24,2048]{1,0:T(8,128)(2,1)S(1)}, bf16[24,2048]{1,0:T(8,128)(2,1)S(1)}, u32[]{:S(2)}, u32[]{:S(2)}) collective-permute-start(bf16[24,2048]{1,0:T(8,128)(2,1)S(1)} %get-tuple-element.76), channel_id=1, source_target_pairs={{0,58},{2,60},{4,62},{6,0},{8,2},{10,4},{12,6},{14,8},{16,10},{18,... | collective-permute-start | bytes 294920 | tf_op jit(solution)/shard_map/ppermute | solution.py:121
  386.4 39.8 %collective-permute-start.30 = (bf16[24,2048]{1,0:T(8,128)(2,1)S(1)}, bf16[24,2048]{1,0:T(8,128)(2,1)S(1)}, u32[]{:S(2)}, u32[]{:S(2)}) collective-permute-start(bf16[24,2048]{1,0:T(8,128)(2,1)S(1)} %get-tuple-element.75), channel_id=1, source_target_pairs={{0,6},{2,8},{4,10},{6,12},{8,14},{10,16},{12,18},{14,20},{16,22},{... | collective-permute-start | bytes 294920 | tf_op jit(solution)/shard_map/ppermute | solution.py:121
  390.9 44.6 %collective-permute-start.31 = (bf16[24,2048]{1,0:T(8,128)(2,1)S(1)}, bf16[24,2048]{1,0:T(8,128)(2,1)S(1)}, u32[]{:S(2)}, u32[]{:S(2)}) collective-permute-start(bf16[24,2048]{1,0:T(8,128)(2,1)S(1)} %get-tuple-element.74), channel_id=1, source_target_pairs={{0,56},{2,58},{4,60},{6,62},{8,0},{10,2},{12,4},{14,6},{16,8},{18,... | collective-permute-start | bytes 294920 | tf_op jit(solution)/shard_map/ppermute | solution.py:121
  413.9 24.1 %collective-permute-start.32 = (bf16[24,2048]{1,0:T(8,128)(2,1)S(1)}, bf16[24,2048]{1,0:T(8,128)(2,1)S(1)}, u32[]{:S(2)}, u32[]{:S(2)}) collective-permute-start(bf16[24,2048]{1,0:T(8,128)(2,1)S(1)} %get-tuple-element.73), channel_id=1, source_target_pairs={{0,8},{2,10},{4,12},{6,14},{8,16},{10,18},{12,20},{14,22},{16,24},... | collective-permute-start | bytes 294920 | tf_op jit(solution)/shard_map/ppermute | solution.py:121
  416.1 26.6 %collective-permute-start.33 = (bf16[24,2048]{1,0:T(8,128)(2,1)S(1)}, bf16[24,2048]{1,0:T(8,128)(2,1)S(1)}, u32[]{:S(2)}, u32[]{:S(2)}) collective-permute-start(bf16[24,2048]{1,0:T(8,128)(2,1)S(1)} %get-tuple-element.72), channel_id=1, source_target_pairs={{0,54},{2,56},{4,58},{6,60},{8,62},{10,0},{12,2},{14,4},{16,6},{18... | collective-permute-start | bytes 294920 | tf_op jit(solution)/shard_map/ppermute | solution.py:121
  426.1 21.1 %collective-permute-start.34 = (bf16[24,2048]{1,0:T(8,128)(2,1)S(1)}, bf16[24,2048]{1,0:T(8,128)(2,1)S(1)}, u32[]{:S(2)}, u32[]{:S(2)}) collective-permute-start(bf16[24,2048]{1,0:T(8,128)(2,1)S(1)} %get-tuple-element.71), channel_id=1, source_target_pairs={{0,10},{2,12},{4,14},{6,16},{8,18},{10,20},{12,22},{14,24},{16,26}... | collective-permute-start | bytes 294920 | tf_op jit(solution)/shard_map/ppermute | solution.py:121
  426.2 28.0 %collective-permute-start.35 = (bf16[24,2048]{1,0:T(8,128)(2,1)S(1)}, bf16[24,2048]{1,0:T(8,128)(2,1)S(1)}, u32[]{:S(2)}, u32[]{:S(2)}) collective-permute-start(bf16[24,2048]{1,0:T(8,128)(2,1)S(1)} %get-tuple-element.70), channel_id=1, source_target_pairs={{0,52},{2,54},{4,56},{6,58},{8,60},{10,62},{12,0},{14,2},{16,4},{1... | collective-permute-start | bytes 294920 | tf_op jit(solution)/shard_map/ppermute | solution.py:121
  435.5 22.1 %collective-permute-start.36 = (bf16[24,2048]{1,0:T(8,128)(2,1)S(1)}, bf16[24,2048]{1,0:T(8,128)(2,1)S(1)}, u32[]{:S(2)}, u32[]{:S(2)}) collective-permute-start(bf16[24,2048]{1,0:T(8,128)(2,1)S(1)} %get-tuple-element.69), channel_id=1, source_target_pairs={{0,12},{2,14},{4,16},{6,18},{8,20},{10,22},{12,24},{14,26},{16,28}... | collective-permute-start | bytes 294920 | tf_op jit(solution)/shard_map/ppermute | solution.py:121
  438.0 33.9 %collective-permute-start.37 = (bf16[24,2048]{1,0:T(8,128)(2,1)S(1)}, bf16[24,2048]{1,0:T(8,128)(2,1)S(1)}, u32[]{:S(2)}, u32[]{:S(2)}) collective-permute-start(bf16[24,2048]{1,0:T(8,128)(2,1)S(1)} %get-tuple-element.68), channel_id=1, source_target_pairs={{0,50},{2,52},{4,54},{6,56},{8,58},{10,60},{12,62},{14,0},{16,2},{... | collective-permute-start | bytes 294920 | tf_op jit(solution)/shard_map/ppermute | solution.py:121
  442.7 29.2 %collective-permute-start.38 = (bf16[24,2048]{1,0:T(8,128)(2,1)S(1)}, bf16[24,2048]{1,0:T(8,128)(2,1)S(1)}, u32[]{:S(2)}, u32[]{:S(2)}) collective-permute-start(bf16[24,2048]{1,0:T(8,128)(2,1)S(1)} %get-tuple-element.67), channel_id=1, source_target_pairs={{0,14},{2,16},{4,18},{6,20},{8,22},{10,24},{12,26},{14,28},{16,30}... | collective-permute-start | bytes 294920 | tf_op jit(solution)/shard_map/ppermute | solution.py:121
  447.3 51.2 %collective-permute-start.39 = (bf16[24,2048]{1,0:T(8,128)(2,1)S(1)}, bf16[24,2048]{1,0:T(8,128)(2,1)S(1)}, u32[]{:S(2)}, u32[]{:S(2)}) collective-permute-start(bf16[24,2048]{1,0:T(8,128)(2,1)S(1)} %get-tuple-element.66), channel_id=1, source_target_pairs={{0,48},{2,50},{4,52},{6,54},{8,56},{10,58},{12,60},{14,62},{16,0},... | collective-permute-start | bytes 294920 | tf_op jit(solution)/shard_map/ppermute | solution.py:121
  454.3 45.3 %collective-permute-start.40 = (bf16[24,2048]{1,0:T(8,128)(2,1)S(1)}, bf16[24,2048]{1,0:T(8,128)(2,1)S(1)}, u32[]{:S(2)}, u32[]{:S(2)}) collective-permute-start(bf16[24,2048]{1,0:T(8,128)(2,1)S(1)} %get-tuple-element.65), channel_id=1, source_target_pairs={{0,16},{2,18},{4,20},{6,22},{8,24},{10,26},{12,28},{14,30},{16,32}... | collective-permute-start | bytes 294920 | tf_op jit(solution)/shard_map/ppermute | solution.py:121
  457.7 61.1 %collective-permute-start.41 = (bf16[24,2048]{1,0:T(8,128)(2,1)S(1)}, bf16[24,2048]{1,0:T(8,128)(2,1)S(1)}, u32[]{:S(2)}, u32[]{:S(2)}) collective-permute-start(bf16[24,2048]{1,0:T(8,128)(2,1)S(1)} %get-tuple-element.64), channel_id=1, source_target_pairs={{0,46},{2,48},{4,50},{6,52},{8,54},{10,56},{12,58},{14,60},{16,62}... | collective-permute-start | bytes 294920 | tf_op jit(solution)/shard_map/ppermute | solution.py:121
  471.9 46.9 %collective-permute-start.42 = (bf16[24,2048]{1,0:T(8,128)(2,1)S(1)}, bf16[24,2048]{1,0:T(8,128)(2,1)S(1)}, u32[]{:S(2)}, u32[]{:S(2)}) collective-permute-start(bf16[24,2048]{1,0:T(8,128)(2,1)S(1)} %get-tuple-element.63), channel_id=1, source_target_pairs={{0,18},{2,20},{4,22},{6,24},{8,26},{10,28},{12,30},{14,32},{16,34}... | collective-permute-start | bytes 294920 | tf_op jit(solution)/shard_map/ppermute | solution.py:121
  471.9 55.2 %collective-permute-start.43 = (bf16[24,2048]{1,0:T(8,128)(2,1)S(1)}, bf16[24,2048]{1,0:T(8,128)(2,1)S(1)}, u32[]{:S(2)}, u32[]{:S(2)}) collective-permute-start(bf16[24,2048]{1,0:T(8,128)(2,1)S(1)} %get-tuple-element.62), channel_id=1, source_target_pairs={{0,44},{2,46},{4,48},{6,50},{8,52},{10,54},{12,56},{14,58},{16,60}... | collective-permute-start | bytes 294920 | tf_op jit(solution)/shard_map/ppermute | solution.py:121
  498.5 28.6 %collective-permute-start.44 = (bf16[24,2048]{1,0:T(8,128)(2,1)S(1)}, bf16[24,2048]{1,0:T(8,128)(2,1)S(1)}, u32[]{:S(2)}, u32[]{:S(2)}) collective-permute-start(bf16[24,2048]{1,0:T(8,128)(2,1)S(1)} %get-tuple-element.61), channel_id=1, source_target_pairs={{0,20},{2,22},{4,24},{6,26},{8,28},{10,30},{12,32},{14,34},{16,36}... | collective-permute-start | bytes 294920 | tf_op jit(solution)/shard_map/ppermute | solution.py:121
  499.6 37.5 %collective-permute-start.45 = (bf16[24,2048]{1,0:T(8,128)(2,1)S(1)}, bf16[24,2048]{1,0:T(8,128)(2,1)S(1)}, u32[]{:S(2)}, u32[]{:S(2)}) collective-permute-start(bf16[24,2048]{1,0:T(8,128)(2,1)S(1)} %get-tuple-element.60), channel_id=1, source_target_pairs={{0,42},{2,44},{4,46},{6,48},{8,50},{10,52},{12,54},{14,56},{16,58}... | collective-permute-start | bytes 294920 | tf_op jit(solution)/shard_map/ppermute | solution.py:121
  518.8 45.5 %collective-permute-start.46 = (bf16[24,2048]{1,0:T(8,128)(2,1)S(1)}, bf16[24,2048]{1,0:T(8,128)(2,1)S(1)}, u32[]{:S(2)}, u32[]{:S(2)}) collective-permute-start(bf16[24,2048]{1,0:T(8,128)(2,1)S(1)} %get-tuple-element.59), channel_id=1, source_target_pairs={{0,22},{2,24},{4,26},{6,28},{8,30},{10,32},{12,34},{14,36},{16,38}... | collective-permute-start | bytes 294920 | tf_op jit(solution)/shard_map/ppermute | solution.py:121
  518.8 45.5 %collective-permute-start.25 = (bf16[24,2048]{1,0:T(8,128)(2,1)S(1)}, bf16[24,2048]{1,0:T(8,128)(2,1)S(1)}, u32[]{:S(2)}, u32[]{:S(2)}) collective-permute-start(bf16[24,2048]{1,0:T(8,128)(2,1)S(1)} %get-tuple-element.80), channel_id=1, source_target_pairs={{0,62},{2,0},{4,2},{6,4},{8,6},{10,8},{12,10},{14,12},{16,14},{18,... | collective-permute-start | bytes 294920 | tf_op jit(solution)/shard_map/ppermute | solution.py:121
  527.1 56.4 %collective-permute-start.26 = (bf16[24,2048]{1,0:T(8,128)(2,1)S(1)}, bf16[24,2048]{1,0:T(8,128)(2,1)S(1)}, u32[]{:S(2)}, u32[]{:S(2)}) collective-permute-start(bf16[24,2048]{1,0:T(8,128)(2,1)S(1)} %get-tuple-element.79), channel_id=1, source_target_pairs={{0,2},{2,4},{4,6},{6,8},{8,10},{10,12},{12,14},{14,16},{16,18},{18... | collective-permute-start | bytes 294920 | tf_op jit(solution)/shard_map/ppermute | solution.py:121
  527.1 57.6 %collective-permute-start.27 = (bf16[24,2048]{1,0:T(8,128)(2,1)S(1)}, bf16[24,2048]{1,0:T(8,128)(2,1)S(1)}, u32[]{:S(2)}, u32[]{:S(2)}) collective-permute-start(bf16[24,2048]{1,0:T(8,128)(2,1)S(1)} %get-tuple-element.78), channel_id=1, source_target_pairs={{0,60},{2,62},{4,0},{6,2},{8,4},{10,6},{12,8},{14,10},{16,12},{18,... | collective-permute-start | bytes 294920 | tf_op jit(solution)/shard_map/ppermute | solution.py:121
  537.1 64.9 %collective-permute-start.60 = (bf16[24,2048]{1,0:T(8,128)(2,1)}, bf16[24,2048]{1,0:T(8,128)(2,1)S(1)}, u32[]{:S(2)}, u32[]{:S(2)}) collective-permute-start(bf16[24,2048]{1,0:T(8,128)(2,1)} %get-tuple-element.86), channel_id=1, source_target_pairs={{0,36},{2,38},{4,40},{6,42},{8,44},{10,46},{12,48},{14,50},{16,52}... | collective-permute-start | bytes 294920 | tf_op jit(solution)/shard_map/ppermute | solution.py:121
  564.3 37.7 %collective-permute-start.61 = (bf16[24,2048]{1,0:T(8,128)(2,1)}, bf16[24,2048]{1,0:T(8,128)(2,1)S(1)}, u32[]{:S(2)}, u32[]{:S(2)}) collective-permute-start(bf16[24,2048]{1,0:T(8,128)(2,1)} %get-tuple-element.85), channel_id=1, source_target_pairs={{0,28},{2,30},{4,32},{6,34},{8,36},{10,38},{12,40},{14,42},{16,44}... | collective-permute-start | bytes 294920 | tf_op jit(solution)/shard_map/ppermute | solution.py:121
  564.3 53.7 %collective-permute-start.62 = (bf16[24,2048]{1,0:T(8,128)(2,1)}, bf16[24,2048]{1,0:T(8,128)(2,1)S(1)}, u32[]{:S(2)}, u32[]{:S(2)}) collective-permute-start(bf16[24,2048]{1,0:T(8,128)(2,1)} %get-tuple-element.84), channel_id=1, source_target_pairs={{0,34},{2,36},{4,38},{6,40},{8,42},{10,44},{12,46},{14,48},{16,50}... | collective-permute-start | bytes 294920 | tf_op jit(solution)/shard_map/ppermute | solution.py:121
  583.5 40.2 %collective-permute-start.63 = (bf16[24,2048]{1,0:T(8,128)(2,1)}, bf16[24,2048]{1,0:T(8,128)(2,1)S(1)}, u32[]{:S(2)}, u32[]{:S(2)}) collective-permute-start(bf16[24,2048]{1,0:T(8,128)(2,1)} %get-tuple-element.83), channel_id=1, source_target_pairs={{0,30},{2,32},{4,34},{6,36},{8,38},{10,40},{12,42},{14,44},{16,46}... | collective-permute-start | bytes 294920 | tf_op jit(solution)/shard_map/ppermute | solution.py:121
  584.8 63.8 %collective-permute-start.64 = (bf16[24,2048]{1,0:T(8,128)(2,1)}, bf16[24,2048]{1,0:T(8,128)(2,1)S(1)}, u32[]{:S(2)}, u32[]{:S(2)}) collective-permute-start(bf16[24,2048]{1,0:T(8,128)(2,1)} %get-tuple-element.82), channel_id=1, source_target_pairs={{0,32},{2,34},{4,36},{6,38},{8,40},{10,42},{12,44},{14,46},{16,48}... | collective-permute-start | bytes 294920 | tf_op jit(solution)/shard_map/ppermute | solution.py:121
  (13 other events, 596.1 us)
